TPU v7x, 32 devices: a whole 2x2x4 slice. The times are simulated.
32 devices in a mesh: dp: 4 (over y, x), kv: 4 (over z), tp: 2 (over core).
Axes of the slice: x: 2, y: 2, z: 4, core: 2. Of those that a mesh axis runs over, the one named last changes fastest.
Arguments:
- tokens: bfloat16 [192, 2048], P(('dp', 'tp'), 'kv'), may hold values from -8 to 8
- mix_gain: float32 [2048], replicated, may hold values from 0.1 to 1.9
- w_gate: bfloat16 [2048, 4096], P(None, 'kv'), may hold values from -0.125 to 0.125
- w_value: bfloat16 [2048, 4096], P(None, 'kv'), may hold values from -0.125 to 0.125
- w_maps: bfloat16 [2048, 16384], P(None, 'kv'), may hold values from -0.125 to 0.125
- w_step: bfloat16 [2048, 64], replicated, may hold values from -0.125 to 0.125
- conv_value: float32 [4, 4096], P(None, 'kv'), may hold values from -0.5 to 0.5
- conv_maps: float32 [4, 16384], P(None, 'kv'), may hold values from -0.5 to 0.5
- past_value: bfloat16 [192, 3, 4096], P(('dp', 'tp'), None, 'kv'), may hold values from -6 to 6
- past_maps: bfloat16 [192, 3, 16384], P(('dp', 'tp'), None, 'kv'), may hold values from -6 to 6
- step_bias: float32 [64], P('kv'), may hold values from -3 to 0
- decay_log: float32 [64], P('kv'), may hold values from 0 to 2.77
- skip_gain: float32 [64], P('kv'), may hold values from 0.1 to 1.9
- head_gain: float32 [4096], P('kv'), may hold values from 0.1 to 1.9
- state: float32 [192, 64, 64, 128], P(('dp', 'tp'), 'kv'), may hold values from -2 to 2
- w_out: bfloat16 [4096, 2048], P('kv'), may hold values from -0.125 to 0.125
- mlp_gain: float32 [2048], replicated, may hold values from 0.1 to 1.9
- w_up: bfloat16 [2048, 8192], P(None, 'kv'), may hold values from -0.125 to 0.125
- w_down: bfloat16 [8192, 2048], P('kv'), may hold values from -0.09375 to 0.09375
Outputs:
- layer_out: bfloat16 [192, 2048], P(('dp', 'tp'), 'kv')
- state_next: float32 [192, 64, 64, 128], P(('dp', 'tp'), 'kv')
- value_tail: bfloat16 [192, 3, 4096], P(('dp', 'tp'), None, 'kv')
- maps_tail: bfloat16 [192, 3, 16384], P(('dp', 'tp'), None, 'kv')
All inputs are finite; a program needn't handle non-finite values.
Results may differ from a plain program's by a relative error of at most 0.0081.
Values may be sent and summed in bfloat16 or wider, within the bound.
A program may use at most 128 MiB of HBM per device.

v0:
```python
import functools

import jax
import jax.numpy as jnp
from jax import lax
from jax.experimental import pallas as pl
from jax.experimental.pallas import tpu as pltpu
from jax.sharding import PartitionSpec as P

HEAD_DIM = 64
STATE = 128
MESH = pl.DeviceIdType.MESH
VMEM_LIMIT = 60 * 1024 * 1024


NORM_EPS = 1e-05
NT = (((1,), (1,)), ((), ()))


def greet(peers, me):
    for d in range(1, peers):
        pl.semaphore_signal(
            pltpu.get_barrier_semaphore(),
            inc=1,
            device_id={"kv": lax.rem(me + d, peers)},
            device_id_type=MESH,
        )


def all_here(peers):
    pl.semaphore_wait(pltpu.get_barrier_semaphore(), peers - 1)


def far_first(peers):
    return sorted(range(1, peers), key=lambda d: -min(d, peers - d))


def push(src, dst, send_sem, recv_sem, target):
    return pltpu.make_async_remote_copy(
        src_ref=src,
        dst_ref=dst,
        send_sem=send_sem,
        recv_sem=recv_sem,
        device_id={"kv": target},
        device_id_type=MESH,
    )


def project_kernel(
    peers,
    tokens,
    gain,
    w_step,
    bias,
    decay_log,
    w_gate,
    w_value,
    w_maps,
    gate_out,
    value_out,
    maps_out,
    step_out,
    decay_out,
    slots,
    weights,
    acc,
    w_sem,
    send_sem,
    recv_sem,
):
    me = lax.axis_index("kv")
    rows, part = tokens.shape
    chunks, width = weights.shape[1], weights.shape[3]
    heads = decay_out.shape[1]
    inner = value_out.shape[1]
    greet(peers, me)

    for d in [0] + far_first(peers)[::-1]:
        start = pl.multiple_of(lax.rem(me + d, peers) * part, part)
        for k, ref in enumerate((w_gate, w_value)):
            pltpu.make_async_copy(
                ref.at[pl.ds(start, part), :],
                weights.at[d, 0, :, pl.ds(k * inner, inner)],
                w_sem.at[d, 0],
            ).start()
        for c in range(1, chunks):
            pltpu.make_async_copy(
                w_maps.at[pl.ds(start, part), pl.ds((c - 1) * width, width)],
                weights.at[d, c],
                w_sem.at[d, c],
            ).start()

    all_here(peers)
    sends = []
    for d in far_first(peers):
        cp = push(
            tokens,
            slots.at[peers - d],
            send_sem.at[d],
            recv_sem.at[peers - d],
            lax.rem(me + d, peers),
        )
        cp.start()
        sends.append(cp)

    squares = jnp.zeros((rows, 1), jnp.float32)
    step_pre = jnp.zeros((2 * rows, w_step.shape[0]), jnp.float32)
    for d in [0] + far_first(peers)[::-1]:
        start = pl.multiple_of(lax.rem(me + d, peers) * part, part)
        if d == 0:
            raw = tokens[...]
        else:
            push(tokens, slots.at[d], send_sem.at[d], recv_sem.at[d], me).wait_recv()
            raw = slots[d]
        wide = raw.astype(jnp.float32)
        squares = squares + jnp.sum(wide * wide, axis=1, keepdims=True)
        scaled = wide * gain[:, pl.ds(start, part)]
        high = scaled.astype(jnp.bfloat16).astype(jnp.float32)
        scaled = jnp.concatenate([high, scaled - high], axis=0).astype(jnp.bfloat16)
        step_pre = step_pre + lax.dot_general(
            scaled, w_step[:, pl.ds(start, part)], NT, preferred_element_type=jnp.float32
        )

        for c in range(chunks):
            pltpu.make_async_copy(
                w_maps.at[pl.ds(0, part), pl.ds(0, width)], weights.at[d, c], w_sem.at[d, c]
            ).wait()
            out = jnp.dot(scaled, weights[d, c], preferred_element_type=jnp.float32)
            out = out[:rows] + out[rows:]
            acc[c] = out if d == 0 else acc[c] + out

    inv = lax.rsqrt(squares / (peers * part) + NORM_EPS)
    for c in range(chunks):
        total = acc[c] * inv
        if c == 0:
            gate_out[...] = total[:, :inner]
            value_out[...] = total[:, inner:].astype(jnp.bfloat16)
        else:
            maps_out[:, (c - 1) * width : c * width] = total.astype(jnp.bfloat16)
    step_pre = (step_pre[:rows] + step_pre[rows:]) * inv
    own = step_pre[:, :heads]
    for j in range(1, peers):
        own = jnp.where(me == j, step_pre[:, j * heads : (j + 1) * heads], own)
    own = own + bias[...]
    step = jnp.maximum(own, 0.0) + jnp.log1p(jnp.exp(-jnp.abs(own)))
    decay_out[...] = jnp.exp(-step * jnp.exp(decay_log[...]))
    lane = lax.broadcasted_iota(jnp.int32, (rows, 2 * HEAD_DIM), 1)
    for h in range(0, heads, 2):
        step_out[:, h * HEAD_DIM : (h + 2) * HEAD_DIM] = jnp.where(
            lane < HEAD_DIM, step[:, h : h + 1], step[:, h + 1 : h + 2]
        )
    for cp in sends:
        cp.wait_send()


def project(peers, tokens, mix_gain, w_step, step_bias, decay_log, w_gate, w_value, w_maps):
    rows, part = tokens.shape
    heads = step_bias.shape[0]
    inner, maps = w_value.shape[1], w_maps.shape[1]
    width = 2 * inner
    chunks = 1 + maps // width
    f32 = jnp.float32
    vmem = pl.BlockSpec(memory_space=pltpu.VMEM)
    hbm = pl.BlockSpec(memory_space=pl.ANY)
    return pl.pallas_call(
        functools.partial(project_kernel, peers),
        out_shape=(
            jax.ShapeDtypeStruct((rows, inner), f32),
            jax.ShapeDtypeStruct((rows, inner), jnp.bfloat16),
            jax.ShapeDtypeStruct((rows, maps), jnp.bfloat16),
            jax.ShapeDtypeStruct((rows, inner), f32),
            jax.ShapeDtypeStruct((rows, heads), f32),
        ),
        in_specs=[vmem] * 5 + [hbm] * 3,
        out_specs=(vmem,) * 5,
        scratch_shapes=[
            pltpu.VMEM((peers, rows, part), jnp.bfloat16),
            pltpu.VMEM((peers, chunks, part, width), jnp.bfloat16),
            pltpu.VMEM((chunks, rows, width), f32),
            pltpu.SemaphoreType.DMA((peers, chunks)),
            pltpu.SemaphoreType.DMA((peers,)),
            pltpu.SemaphoreType.DMA((peers,)),
        ],
        compiler_params=pltpu.CompilerParams(
            collective_id=0, has_side_effects=True, vmem_limit_bytes=VMEM_LIMIT
        ),
        name="project",
    )(
        tokens,
        mix_gain[None, :],
        w_step.T,
        step_bias[None, :],
        decay_log[None, :],
        w_gate,
        w_value,
        w_maps,
    )


def silu(x):
    return x * jax.nn.sigmoid(x)


def state_kernel(
    decay,
    skip,
    state,
    gate,
    value_new,
    maps_new,
    step,
    past_value,
    past_maps,
    conv_value,
    conv_maps,
    head_gain,
    heads_out,
    state_out,
    value_tail,
    maps_tail,
):
    i = pl.program_id(0)
    rows = state.shape[0]

    def conv(past, new, taps, tail):
        taps_n = past.shape[0]
        total = new[...].astype(jnp.float32) * taps[taps_n : taps_n + 1, :]
        for k in range(taps_n):
            row = past[k]
            total = total + row.astype(jnp.float32) * taps[k : k + 1, :]
            if k > 0:
                tail[k - 1] = row
        tail[taps_n - 1] = new[...]
        return silu(total)

    value_act = conv(past_value, value_new, conv_value, value_tail)
    maps_act = conv(past_maps, maps_new, conv_maps, maps_tail)
    maps_act = maps_act.astype(jnp.bfloat16).astype(jnp.float32)

    scaled = value_act * step[...]
    high = scaled.astype(jnp.bfloat16).astype(jnp.float32)
    both = jnp.concatenate([high, scaled - high], axis=0).T.astype(jnp.bfloat16)
    ins = []
    outs = []
    for hh in range(2):
        at = 2 * hh * STATE
        ins.append(jnp.concatenate([maps_act[:, at : at + STATE]] * 2, axis=0))
        outs.append(maps_act[:, at + STATE : at + 2 * STATE])
    readers = jnp.concatenate(outs, axis=0).astype(jnp.bfloat16)

    row = lax.broadcasted_iota(jnp.int32, (2 * rows, STATE), 0)
    lane = lax.broadcasted_iota(jnp.int32, (2 * rows, STATE), 1)
    seq = jnp.where(row >= rows, row - rows, row)
    owner = jnp.where((row >= rows) == (lane >= HEAD_DIM), seq, -1)
    read = jnp.zeros((2 * rows, 2 * HEAD_DIM), jnp.float32)
    for b in range(0, rows, 2):
        fresh = [None] * 4
        for hh in range(2):
            spread = jnp.concatenate(
                [jnp.where(seq == b + k, ins[hh], 0.0) for k in range(2)], axis=1
            ).astype(jnp.bfloat16)
            written = jnp.dot(
                both[hh * HEAD_DIM : (hh + 1) * HEAD_DIM],
                spread,
                preferred_element_type=jnp.float32,
            )
            for k in range(2):
                new = (
                    decay[b + k, 2 * i + hh] * state[b + k, hh]
                    + written[:, k * STATE : (k + 1) * STATE]
                )
                state_out[b + k, hh] = new
                fresh[2 * k + hh] = new.astype(jnp.bfloat16)
        found = lax.dot_general(
            readers, jnp.concatenate(fresh, axis=0), NT, preferred_element_type=jnp.float32
        )
        for k in range(2):
            read = read + jnp.where(
                owner == b + k, found[:, k * 2 * HEAD_DIM : (k + 1) * 2 * HEAD_DIM], 0.0
            )
    first = lane[:rows] < HEAD_DIM
    read_out = read[:rows] + read[rows:]
    read_out = read_out + jnp.where(first, skip[2 * i], skip[2 * i + 1]) * value_act
    gated = read_out * silu(gate[...])
    square = gated * gated
    low = jnp.sum(jnp.where(first, square, 0.0), axis=1, keepdims=True)
    top = jnp.sum(jnp.where(first, 0.0, square), axis=1, keepdims=True)
    inv = lax.rsqrt(jnp.where(first, low, top) / HEAD_DIM + NORM_EPS)
    heads_out[...] = (gated * inv * head_gain[...]).astype(jnp.bfloat16)


def step_state(
    decay,
    skip_gain,
    state,
    gate,
    value_new,
    maps_new,
    step,
    past_value,
    past_maps,
    conv_value,
    conv_maps,
    head_gain,
):
    rows, heads = state.shape[:2]
    smem = pl.BlockSpec(memory_space=pltpu.SMEM)
    pair = 2 * HEAD_DIM
    wide = 4 * STATE
    taps = conv_value.shape[0]
    past_v = jnp.swapaxes(past_value, 0, 1)
    past_m = jnp.swapaxes(past_maps, 0, 1)
    flat = lambda width: pl.BlockSpec((rows, width), lambda i: (0, i))
    conv_spec = lambda width: pl.BlockSpec((taps, width), lambda i: (0, i))
    past_spec = lambda width: pl.BlockSpec((taps - 1, rows, width), lambda i: (0, 0, i))
    state_spec = pl.BlockSpec((rows, 2, HEAD_DIM, STATE), lambda i: (0, i, 0, 0))
    heads_out, state_next, tail_v, tail_m = pl.pallas_call(
        state_kernel,
        grid=(heads // 2,),
        out_shape=(
            jax.ShapeDtypeStruct((rows, heads * HEAD_DIM), jnp.bfloat16),
            jax.ShapeDtypeStruct(state.shape, jnp.float32),
            jax.ShapeDtypeStruct(past_v.shape, jnp.bfloat16),
            jax.ShapeDtypeStruct(past_m.shape, jnp.bfloat16),
        ),
        in_specs=[
            smem,
            smem,
            state_spec,
            flat(pair),
            flat(pair),
            flat(wide),
            flat(pair),
            past_spec(pair),
            past_spec(wide),
            conv_spec(pair),
            conv_spec(wide),
            pl.BlockSpec((1, pair), lambda i: (0, i)),
        ],
        out_specs=(flat(pair), state_spec, past_spec(pair), past_spec(wide)),
        compiler_params=pltpu.CompilerParams(
            dimension_semantics=("arbitrary",), vmem_limit_bytes=VMEM_LIMIT
        ),
        name="step_state",
    )(
        decay,
        skip_gain,
        state,
        gate,
        value_new,
        maps_new,
        step,
        past_v,
        past_m,
        conv_value,
        conv_maps,
        head_gain[None, :],
    )
    return heads_out, state_next, jnp.swapaxes(tail_v, 0, 1), jnp.swapaxes(tail_m, 0, 1)


def mixer_kernel(
    peers,
    heads,
    tokens,
    gain,
    w_out,
    w_up,
    w_down,
    layer_out,
    out_w,
    up_w,
    down_w,
    sums_a,
    land_a,
    own_hidden,
    hidden,
    up_acc,
    squared,
    sums_b,
    land_b,
    out_sem,
    up_sem,
    down_sem,
    send_a,
    recv_a,
    send_h,
    recv_h,
    send_b,
    recv_b,
):
    me = lax.axis_index("kv")
    rows, part = tokens.shape
    n_up, width = up_w.shape[1], up_w.shape[3]

    def place(d):
        return pl.multiple_of(lax.rem(me + d, peers) * part, part)

    order = far_first(peers) + [0]
    greet(peers, me)
    waits_out, waits_down = {}, {}
    for d in order:
        cp = pltpu.make_async_copy(w_out.at[:, pl.ds(place(d), part)], out_w.at[d], out_sem.at[d])
        cp.start()
        waits_out[d] = cp
    for d in range(peers):
        for c in range(n_up):
            pltpu.make_async_copy(
                w_up.at[pl.ds(place(d), part), pl.ds(c * width, width)],
                up_w.at[d, c],
                up_sem.at[d, c],
            ).start()
    for d in order:
        cp = pltpu.make_async_copy(
            w_down.at[:, pl.ds(place(d), part)], down_w.at[d], down_sem.at[d]
        )
        cp.start()
        waits_down[d] = cp

    pending = []

    def scatter(left, weights, waits, sums, land, send, recv):
        for d in order:
            waits[d].wait()
            piece = jnp.dot(left, weights[d], preferred_element_type=jnp.float32)
            if d == 0:
                total = piece
            else:
                sums[d] = piece.astype(jnp.bfloat16)
                if not pending:
                    all_here(peers)
                cp = push(
                    sums.at[d],
                    land.at[peers - d],
                    send.at[d],
                    recv.at[peers - d],
                    lax.rem(me + d, peers),
                )
                cp.start()
                pending.append(cp)
        for d in range(1, peers):
            push(sums.at[d], land.at[d], send.at[d], recv.at[d], me).wait_recv()
            total = total + land[d].astype(jnp.float32)
        return total

    total = scatter(heads[...], out_w, waits_out, sums_a, land_a, send_a, recv_a)
    mine = (tokens[...].astype(jnp.float32) + total).astype(jnp.bfloat16)
    own_hidden[...] = mine
    for d in range(1, peers):
        cp = push(
            own_hidden,
            hidden.at[peers - d],
            send_h.at[d],
            recv_h.at[peers - d],
            lax.rem(me + d, peers),
        )
        cp.start()
        pending.append(cp)

    squares = jnp.zeros((rows, 1), jnp.float32)
    for d in range(peers):
        if d == 0:
            raw = mine
        else:
            push(own_hidden, hidden.at[d], send_h.at[d], recv_h.at[d], me).wait_recv()
            raw = hidden[d]
        wide = raw.astype(jnp.float32)
        squares = squares + jnp.sum(wide * wide, axis=1, keepdims=True)
        scaled = wide * gain[:, pl.ds(place(d), part)]
        high = scaled.astype(jnp.bfloat16).astype(jnp.float32)
        scaled = jnp.concatenate([high, scaled - high], axis=0).astype(jnp.bfloat16)

        def chunk(c, carry, d=d, scaled=scaled):
            pltpu.make_async_copy(
                w_up.at[pl.ds(0, part), pl.ds(0, width)], up_w.at[d, c], up_sem.at[d, c]
            ).wait()
            out = jnp.dot(scaled, up_w[d, c], preferred_element_type=jnp.float32)
            out = out[:rows] + out[rows:]
            up_acc[c] = out if d == 0 else up_acc[c] + out
            return carry

        lax.fori_loop(0, n_up, chunk, 0)

    inv = lax.rsqrt(squares / (peers * part) + NORM_EPS)
    for c in range(n_up):
        up = jnp.maximum(up_acc[c] * inv, 0.0)
        squared[:, c * width : (c + 1) * width] = (up * up).astype(jnp.bfloat16)
    total = scatter(squared[...], down_w, waits_down, sums_b, land_b, send_b, recv_b)
    layer_out[...] = (mine.astype(jnp.float32) + total).astype(jnp.bfloat16)
    for cp in pending:
        cp.wait_send()


def mix_channels(peers, heads_out, tokens, mlp_gain, w_out, w_up, w_down):
    rows, part = tokens.shape
    inner, hid = w_out.shape[0], w_up.shape[1]
    width = min(2048, hid)
    f32, bf16 = jnp.float32, jnp.bfloat16
    vmem = pl.BlockSpec(memory_space=pltpu.VMEM)
    hbm = pl.BlockSpec(memory_space=pl.ANY)
    sems = pltpu.SemaphoreType.DMA((peers,))
    return pl.pallas_call(
        functools.partial(mixer_kernel, peers),
        out_shape=jax.ShapeDtypeStruct((rows, part), bf16),
        in_specs=[vmem] * 3 + [hbm] * 3,
        out_specs=vmem,
        scratch_shapes=[
            pltpu.VMEM((peers, inner, part), bf16),
            pltpu.VMEM((peers, hid // width, part, width), bf16),
            pltpu.VMEM((peers, hid, part), bf16),
            pltpu.VMEM((peers, rows, part), bf16),
            pltpu.VMEM((peers, rows, part), bf16),
            pltpu.VMEM((rows, part), bf16),
            pltpu.VMEM((peers, rows, part), bf16),
            pltpu.VMEM((hid // width, rows, width), f32),
            pltpu.VMEM((rows, hid), bf16),
            pltpu.VMEM((peers, rows, part), bf16),
            pltpu.VMEM((peers, rows, part), bf16),
            sems,
            pltpu.SemaphoreType.DMA((peers, hid // width)),
            sems,
            sems,
            sems,
            sems,
            sems,
            sems,
            sems,
        ],
        compiler_params=pltpu.CompilerParams(
            collective_id=1, has_side_effects=True, vmem_limit_bytes=VMEM_LIMIT
        ),
        name="mix_channels",
    )(heads_out, tokens, mlp_gain[None, :], w_out, w_up, w_down)


def local_kernels(
    peers,
    tokens,
    mix_gain,
    w_gate,
    w_value,
    w_maps,
    w_step,
    conv_value,
    conv_maps,
    past_value,
    past_maps,
    step_bias,
    decay_log,
    skip_gain,
    head_gain,
    state,
    w_out,
    mlp_gain,
    w_up,
    w_down,
):
    gate, value_new, maps_new, step, decay = project(
        peers, tokens, mix_gain, w_step, step_bias, decay_log, w_gate, w_value, w_maps
    )
    heads_out, state_next, value_tail, maps_tail = step_state(
        decay,
        skip_gain,
        state,
        gate,
        value_new,
        maps_new,
        step,
        past_value,
        past_maps,
        conv_value,
        conv_maps,
        head_gain,
    )
    layer_out = mix_channels(peers, heads_out, tokens, mlp_gain, w_out, w_up, w_down)
    return layer_out, state_next, value_tail, maps_tail


def kernels_fit(peers, tokens, state, w_maps, w_up):
    rows, part = tokens.shape
    heads = state.shape[1]
    inner = heads * HEAD_DIM
    width = min(1024, inner)
    held = 2 * tokens.shape[1] * peers * (2 * inner + w_maps.shape[1])
    return (
        peers > 1
        and rows % 8 == 0
        and part % 128 == 0
        and heads % 2 == 0
        and w_maps.shape[1] == heads * 2 * STATE
        and inner % width == 0
        and width % 128 == 0
        and w_up.shape[1] % min(2048, w_up.shape[1]) == 0
        and w_up.shape[1] % 128 == 0
        and held <= 32 * 1024 * 1024
    )


def rms_rows(matrix, gain_vec):
    widened = matrix.astype(jnp.float32)
    inv_scale = lax.rsqrt(jnp.mean(widened * widened, axis=-1, keepdims=True) + NORM_EPS)
    return (widened * inv_scale * gain_vec).astype(jnp.bfloat16)


def short_conv(past_rows, newest, kernel):
    window = jnp.concatenate([past_rows, newest[:, None, :]], axis=1)
    summed = jnp.sum(window.astype(jnp.float32) * kernel[None], axis=1)
    return (jax.nn.silu(summed), window[:, 1:, :])


def local(
    tokens,
    mix_gain,
    w_gate,
    w_value,
    w_maps,
    w_step,
    conv_value,
    conv_maps,
    past_value,
    past_maps,
    step_bias,
    decay_log,
    skip_gain,
    head_gain,
    state,
    w_out,
    mlp_gain,
    w_up,
    w_down,
):
    whole_rows = lax.all_gather(tokens, "kv", axis=1, tiled=True)
    batch_rows = whole_rows.shape[0]
    heads_here = state.shape[1]
    head_start = lax.axis_index("kv") * heads_here
    normed = rms_rows(whole_rows, mix_gain)
    gate_pre = jnp.dot(normed, w_gate, preferred_element_type=jnp.float32)
    step_cols = lax.dynamic_slice_in_dim(w_step, head_start, heads_here, 1)
    step_pre = jnp.dot(normed, step_cols, preferred_element_type=jnp.float32)
    value_new = jnp.dot(normed, w_value, preferred_element_type=jnp.float32).astype(jnp.bfloat16)
    maps_new = jnp.dot(normed, w_maps, preferred_element_type=jnp.float32).astype(jnp.bfloat16)
    value_act, value_tail = short_conv(past_value, value_new, conv_value)
    maps_act, maps_tail = short_conv(past_maps, maps_new, conv_maps)
    maps_act = lax.optimization_barrier(maps_act.astype(jnp.bfloat16))
    grouped = maps_act.astype(jnp.float32).reshape(batch_rows, -1, 2, STATE)
    per_group = heads_here // grouped.shape[1]
    in_map = jnp.repeat(grouped[:, :, 0], per_group, axis=1)
    out_map = jnp.repeat(grouped[:, :, 1], per_group, axis=1)
    head_values = value_act.reshape(batch_rows, heads_here, HEAD_DIM)
    step_size = jax.nn.softplus(step_pre + step_bias)
    decay_rate = jnp.exp(-step_size * jnp.exp(decay_log))
    written = (step_size[:, :, None] * head_values)[:, :, :, None] * in_map[:, :, None, :]
    state_next = decay_rate[:, :, None, None] * state + written
    read_out = (
        jnp.sum(state_next * out_map[:, :, None, :], axis=-1)
        + skip_gain[None, :, None] * head_values
    )
    gated_heads = read_out * jax.nn.silu(gate_pre.reshape(batch_rows, heads_here, HEAD_DIM))
    inv_scale = lax.rsqrt(jnp.mean(gated_heads * gated_heads, axis=-1, keepdims=True) + NORM_EPS)
    heads_out = gated_heads * inv_scale * head_gain.reshape(heads_here, HEAD_DIM)
    heads_out = heads_out.reshape(batch_rows, heads_here * HEAD_DIM).astype(jnp.bfloat16)
    partial_value = jnp.dot(heads_out, w_out, preferred_element_type=jnp.float32)
    own_part = lax.psum_scatter(partial_value, "kv", scatter_dimension=1, tiled=True)
    own_hidden = lax.optimization_barrier(
        (tokens.astype(jnp.float32) + own_part).astype(jnp.bfloat16)
    )
    hidden = lax.all_gather(own_hidden, "kv", axis=1, tiled=True)
    normed_mlp = rms_rows(hidden, mlp_gain)
    squared = jnp.square(jax.nn.relu(jnp.dot(normed_mlp, w_up, preferred_element_type=jnp.float32)))
    squared = squared.astype(jnp.bfloat16)
    partial_mlp = jnp.dot(squared, w_down, preferred_element_type=jnp.float32)
    mlp_part = lax.psum_scatter(partial_mlp, "kv", scatter_dimension=1, tiled=True)
    layer_out = (own_hidden.astype(jnp.float32) + mlp_part).astype(jnp.bfloat16)
    return (layer_out, state_next, value_tail, maps_tail)


def solution(mesh):
    in_specs = (
        P(("dp", "tp"), "kv"),
        P(),
        P(None, "kv"),
        P(None, "kv"),
        P(None, "kv"),
        P(),
        P(None, "kv"),
        P(None, "kv"),
        P(("dp", "tp"), None, "kv"),
        P(("dp", "tp"), None, "kv"),
        P("kv"),
        P("kv"),
        P("kv"),
        P("kv"),
        P(("dp", "tp"), "kv", None, None),
        P("kv", None),
        P(),
        P(None, "kv"),
        P("kv", None),
    )
    out_specs = (
        P(("dp", "tp"), "kv"),
        P(("dp", "tp"), "kv", None, None),
        P(("dp", "tp"), None, "kv"),
        P(("dp", "tp"), None, "kv"),
    )
    peers = mesh.shape["kv"]

    def device_part(*args):
        if kernels_fit(peers, args[0], args[14], args[4], args[17]):
            return local_kernels(peers, *args)
        return local(*args)

    return jax.shard_map(
        device_part, mesh=mesh, in_specs=in_specs, out_specs=out_specs, check_vma=False
    )
```

profile of v0, /device:TPU:0, one launch (start us, length us, event | category | flops | bytes accessed | tf_op | source)
XLA Modules:
  0.0 52.3 jit_solution(6606926298884658887)
XLA Ops:
  0.6 14.3 %project.1 = (f32[24,1024]{1,0:T(8,128)}, bf16[24,1024]{1,0:T(8,128)(2,1)}, bf16[24,4096]{1,0:T(8,128)(2,1)}, f32[24,1024]{1,0:T(8,128)}, f32[24,16]{1,0:T(8,128)}) custom-call(bf16[24,512]{1,0:T(8,128)(2,1)} %tokens.3, f32[1,2048]{1,0:T(1,128)} %bitcast.13, bf16[64,2048]{1,0:T(8,128)(2,1)} %bitcast.11, f32[1,16]{1,0:T(1,128)} %bitcast.16, ...), custom_call_target="tpu_custom_call" | custom-call | tf_op jit(solution)/shard_map/project/pallas_call | solution.py:165
  14.9 15.2 %step_state.1 = (bf16[24,1024]{1,0:T(8,128)(2,1)}, f32[24,16,64,128]{3,2,1,0:T(8,128)}, bf16[3,24,1024]{2,1,0:T(8,128)(2,1)}, bf16[3,24,4096]{2,1,0:T(8,128)(2,1)}) custom-call(f32[24,16]{1,0:T(8,128)} %get-tuple-element.13.decay, f32[16]{0:T(128)} %skip.1, f32[24,16,64,128]{3,2,1,0:T(8,128)} %state.1, f32[24,1024]{1,0:T(8,128)} %get-tuple-element.14.gate, ...), custom_call_target="tpu_custom_call" | custom-call | tf_op jit(solution)/shard_map/step_state/pallas_call | solution.py:317
  30.1 20.9 %mix_channels.1 = bf16[24,512]{1,0:T(8,128)(2,1)} custom-call(bf16[24,1024]{1,0:T(8,128)(2,1)} %get-tuple-element.18.heads, bf16[24,512]{1,0:T(8,128)(2,1)} %tokens.3, f32[1,2048]{1,0:T(1,128)} %bitcast.14, bf16[1024,2048]{1,0:T(8,128)(2,1)} %w_out.1, bf16[2048,2048]{1,0:T(8,128)(2,1)} %w_up.1, bf16[2048,2048]{1,0:T(8,128)(2,1)} %w_down.1), custom_call_target="tpu_custom_call" | custom-call | tf_op jit(solution)/shard_map/mix_channels/pallas_call | solution.py:502
  50.9 1.3 %copy.24 = bf16[24,512]{1,0:T(8,128)(2,1)} copy(bf16[24,512]{1,0:T(8,128)(2,1)} %mix_channels.1) | data formatting | bytes 49152
where the time goes:
time: 52.6 us; the launch traced here: 52.3 us
  Pallas kernels  50.3 us (96%)
  local copies, waits for them, and re-layouts  1.35 us (3%)
  between operations  0.65 us (1%)
    pallas_call x1, Pallas kernels, mix_channels(): pl.pallas_call(functools.partial(mixer_kernel, peers), out_shape=jax.Shap...  20.9 us
    pallas_call x1, Pallas kernels, step_state(): pl.pallas_call(state_kernel, grid=(heads // 2,), out_shape=(jax.ShapeDtyp...  15.2 us
    pallas_call x1, Pallas kernels, project(): pl.pallas_call(functools.partial(project_kernel, peers), out_shape=(jax.S...  14.3 us
    unnamed x1, local copies, waits for them, and re-layouts  1.35 us

commit v1 on v0

v1 whole, which is shorter than its diff:
```python
import functools

import jax
import jax.numpy as jnp
from jax import lax
from jax.experimental import pallas as pl
from jax.experimental.pallas import tpu as pltpu
from jax.sharding import PartitionSpec as P

HEAD_DIM = 64
STATE = 128
MESH = pl.DeviceIdType.MESH


NORM_EPS = 1e-05
NT = (((1,), (1,)), ((), ()))


def partner(me, d):
    other = me
    bit = 1
    while bit <= d:
        if d & bit:
            other = other + bit - 2 * bit * lax.rem(lax.div(me, bit), 2)
        bit *= 2
    return other


def greet(peers, me):
    for d in range(1, peers):
        pl.semaphore_signal(
            pltpu.get_barrier_semaphore(),
            inc=1,
            device_id={"kv": partner(me, d)},
            device_id_type=MESH,
        )


def all_here(peers):
    pl.semaphore_wait(pltpu.get_barrier_semaphore(), peers - 1)


def far_first(peers):
    return list(range(1, peers))[::-1]


def push(src, dst, send_sem, recv_sem, target):
    return pltpu.make_async_remote_copy(
        src_ref=src,
        dst_ref=dst,
        send_sem=send_sem,
        recv_sem=recv_sem,
        device_id={"kv": target},
        device_id_type=MESH,
    )


def in_hbm(*arrays):
    return [pltpu.with_memory_space_constraint(x, pltpu.HBM) for x in arrays]


def in_vmem(*arrays):
    return [pltpu.with_memory_space_constraint(x, pltpu.VMEM) for x in arrays]


def silu(x):
    return x * jax.nn.sigmoid(x)


def split(x):
    high = x.astype(jnp.bfloat16).astype(jnp.float32)
    return high, x - high


def project_kernel(
    peers,
    tokens_in,
    gain_in,
    w_step_in,
    bias_in,
    decay_log_in,
    skip_in,
    conv_value_in,
    conv_maps_in,
    w_gate,
    w_value,
    w_maps,
    past_value_in,
    past_maps_in,
    state_in,
    gate_out,
    direct_out,
    value_out,
    maps_out,
    act_out,
    spread_out,
    decay_out,
    past_value,
    past_maps,
    state_out,
    tokens,
    gain,
    w_step,
    bias,
    decay_log,
    skip,
    conv_value,
    conv_maps,
    slots,
    weights,
    acc,
    small_sem,
    w_sem,
    state_sem,
    send_sem,
    recv_sem,
):
    me = lax.axis_index("kv")
    rows, part = tokens.shape
    chunks, width = weights.shape[1], weights.shape[3]
    heads = bias.shape[1]
    inner = value_out.shape[1]
    pair = 2 * HEAD_DIM
    taps = past_value.shape[0]
    greet(peers, me)

    def place(d):
        return pl.multiple_of(partner(me, d) * part, part)

    small = []
    for k, (src, dst) in enumerate(
        (
            (tokens_in, tokens),
            (gain_in, gain),
            (w_step_in, w_step),
            (bias_in, bias),
            (decay_log_in, decay_log),
            (skip_in, skip),
            (conv_value_in, conv_value),
            (conv_maps_in, conv_maps),
            (past_value_in, past_value),
            (past_maps_in, past_maps),
        )
    ):
        small.append(pltpu.make_async_copy(src, dst, small_sem.at[k]))
    def load_weights(d):
        for k, ref in enumerate((w_gate, w_value)):
            pltpu.make_async_copy(
                ref.at[pl.ds(place(d), part), :],
                weights.at[d, 0, :, pl.ds(k * inner, inner)],
                w_sem.at[d, 0],
            ).start(priority=1)
        for c in range(1, chunks):
            pltpu.make_async_copy(
                w_maps.at[pl.ds(place(d), part), pl.ds((c - 1) * width, width)],
                weights.at[d, c],
                w_sem.at[d, c],
            ).start(priority=1)

    for cp in small[:3]:
        cp.start()
    load_weights(0)
    small[0].wait()
    all_here(peers)
    sends = []
    for d in far_first(peers):
        cp = push(tokens, slots.at[d], send_sem.at[d], recv_sem.at[d], partner(me, d))
        cp.start()
        sends.append(cp)
    for cp in small[3:]:
        cp.start()
    for d in range(1, peers):
        load_weights(d)
    blocks = state_sem.shape[0]
    step_rows = rows // blocks
    state_copies = []
    for k in range(blocks):
        at = pl.ds(k * step_rows, step_rows)
        cp = pltpu.make_async_copy(state_in.at[at], state_out.at[at], state_sem.at[k])
        cp.start(priority=1)
        state_copies.append(cp)
    for cp in small[1:]:
        cp.wait()

    lane = lax.broadcasted_iota(jnp.int32, (rows, pair), 1)

    def by_head(table, h):
        return jnp.where(lane < HEAD_DIM, table[:, h : h + 1], table[:, h + 1 : h + 2])

    squares = jnp.zeros((rows, 1), jnp.float32)
    step_pre = jnp.zeros((2 * rows, w_step.shape[0]), jnp.float32)
    for d in range(peers):
        if d == 0:
            raw = tokens[...]
        else:
            push(tokens, slots.at[d], send_sem.at[d], recv_sem.at[d], me).wait_recv()
            raw = slots[d]
        wide = raw.astype(jnp.float32)
        squares = squares + jnp.sum(wide * wide, axis=1, keepdims=True)
        scaled = jnp.concatenate(split(wide * gain[:, pl.ds(place(d), part)]), axis=0)
        scaled = scaled.astype(jnp.bfloat16)
        step_pre = step_pre + lax.dot_general(
            scaled, w_step[:, pl.ds(place(d), part)], NT, preferred_element_type=jnp.float32
        )
        last = d == peers - 1
        if last:
            inv = lax.rsqrt(squares / (peers * part) + NORM_EPS)
            step_pre = (step_pre[:rows] + step_pre[rows:]) * inv
            own = step_pre[:, :heads]
            for j in range(1, peers):
                own = jnp.where(me == j, step_pre[:, j * heads : (j + 1) * heads], own)
            own = own + bias[...]
            step = jnp.maximum(own, 0.0) + jnp.log1p(jnp.exp(-jnp.abs(own)))
            decay = jnp.exp(-step * jnp.exp(decay_log[...]))
            for h in range(heads):
                decay_out[h] = jnp.broadcast_to(decay[:, h : h + 1], (rows, STATE))

        for c in range(chunks):
            pltpu.make_async_copy(
                w_maps.at[pl.ds(0, part), pl.ds(0, width)], weights.at[d, c], w_sem.at[d, c]
            ).wait()
            out = jnp.dot(scaled, weights[d, c], preferred_element_type=jnp.float32)
            out = out[:rows] + out[rows:]
            total = out if d == 0 else acc[c] + out
            if not last:
                acc[c] = total
                continue
            total = total * inv

            def conv(new, past, at, cols, table):
                summed = new.astype(jnp.float32) * table[taps : taps + 1, at : at + cols]
                for k in range(taps):
                    row = past[k, :, at : at + cols].astype(jnp.float32)
                    summed = summed + row * table[k : k + 1, at : at + cols]
                return silu(summed)

            if c == 0:
                gate_out[...] = silu(total[:, :inner])
                new = total[:, inner:].astype(jnp.bfloat16)
                value_out[...] = new
                act = conv(new, past_value, 0, inner, conv_value)
                for h in range(0, heads, 2):
                    at = h * HEAD_DIM
                    one = act[:, at : at + pair]
                    direct_out[:, at : at + pair] = by_head(skip, h) * one
                    one = one * by_head(step, h)
                    both = jnp.concatenate(split(one), axis=0)
                    blank = jnp.zeros((STATE - 4 * rows, HEAD_DIM), jnp.float32)
                    stack = jnp.concatenate(
                        [both[:, :HEAD_DIM], both[:, HEAD_DIM:], blank], axis=0
                    )
                    spread_out[h // 2] = stack.T.astype(jnp.bfloat16)
            else:
                at = (c - 1) * width
                new = total.astype(jnp.bfloat16)
                maps_out[:, at : at + width] = new
                act = conv(new, past_maps, at, width, conv_maps)
                act_out[:, at : at + width] = act.astype(jnp.bfloat16)

    for cp in state_copies:
        cp.wait()
    for cp in sends:
        cp.wait_send()


def project(
    peers,
    tokens,
    mix_gain,
    w_step,
    step_bias,
    decay_log,
    skip_gain,
    conv_value,
    conv_maps,
    w_gate,
    w_value,
    w_maps,
    past_value,
    past_maps,
    state,
):
    rows, part = tokens.shape
    heads = step_bias.shape[0]
    inner, maps = w_value.shape[1], w_maps.shape[1]
    width = 2 * inner
    chunks = 1 + maps // width
    f32, bf16 = jnp.float32, jnp.bfloat16
    blocks = next(k for k in (8, 6, 4, 3, 2, 1) if rows % k == 0)
    vmem = pl.BlockSpec(memory_space=pltpu.VMEM)
    hbm = pl.BlockSpec(memory_space=pl.ANY)
    return pl.pallas_call(
        functools.partial(project_kernel, peers),
        out_shape=(
            pltpu.VMEM((rows, inner), f32),
            pltpu.VMEM((rows, inner), f32),
            pltpu.VMEM((rows, inner), bf16),
            pltpu.VMEM((rows, maps), bf16),
            pltpu.VMEM((rows, maps), bf16),
            pltpu.VMEM((heads // 2, HEAD_DIM, STATE), bf16),
            pltpu.VMEM((heads, rows, STATE), f32),
            pltpu.VMEM(past_value.shape, bf16),
            pltpu.VMEM(past_maps.shape, bf16),
            pltpu.VMEM(state.shape, f32),
        ),
        in_specs=[hbm] * 14,
        out_specs=(vmem,) * 10,
        scratch_shapes=[
            pltpu.VMEM((rows, part), bf16),
            pltpu.VMEM((1, peers * part), f32),
            pltpu.VMEM((w_step.shape[1], peers * part), bf16),
            pltpu.VMEM((1, heads), f32),
            pltpu.VMEM((1, heads), f32),
            pltpu.VMEM((1, heads), f32),
            pltpu.VMEM(conv_value.shape, f32),
            pltpu.VMEM(conv_maps.shape, f32),
            pltpu.VMEM((peers, rows, part), bf16),
            pltpu.VMEM((peers, chunks, part, width), bf16),
            pltpu.VMEM((chunks, rows, width), f32),
            pltpu.SemaphoreType.DMA((10,)),
            pltpu.SemaphoreType.DMA((peers, chunks)),
            pltpu.SemaphoreType.DMA((blocks,)),
            pltpu.SemaphoreType.DMA((peers,)),
            pltpu.SemaphoreType.DMA((peers,)),
        ],
        compiler_params=pltpu.CompilerParams(
            collective_id=0, has_side_effects=True, vmem_limit_bytes=28 * 1024 * 1024
        ),
        name="project",
    )(
        *in_hbm(
            tokens,
            mix_gain[None, :],
            w_step.T,
            step_bias[None, :],
            decay_log[None, :],
            skip_gain[None, :],
            conv_value,
            conv_maps,
            w_gate,
            w_value,
            w_maps,
            past_value,
            past_maps,
            state,
        )
    )


def state_kernel(
    gate,
    direct,
    value_new,
    maps_new,
    maps_act,
    spread,
    decay,
    past_value,
    past_maps,
    state,
    head_gain_in,
    w_out_in,
    heads_out,
    w_out,
    state_out,
    value_tail,
    maps_tail,
    fresh,
    pick,
    read,
    head_gain,
    in_sem,
    tail_sem,
    out_sem,
):
    rows, heads = state.shape[:2]
    taps = past_value.shape[0]
    pair = 2 * HEAD_DIM
    wide = 4 * STATE
    group = 4
    loads = [
        pltpu.make_async_copy(head_gain_in, head_gain, in_sem.at[0]),
        pltpu.make_async_copy(w_out_in, w_out, in_sem.at[1]),
    ]
    tails = []
    for k, (past, new, tail) in enumerate(
        ((past_value, value_new, value_tail), (past_maps, maps_new, maps_tail))
    ):
        tails.append(
            pltpu.make_async_copy(
                past.at[pl.ds(1, taps - 1)], tail.at[pl.ds(0, taps - 1)], tail_sem.at[k, 0]
            )
        )
        tails.append(pltpu.make_async_copy(new, tail.at[taps - 1], tail_sem.at[k, 1]))
    for cp in loads + tails:
        cp.start()

    lane = lax.broadcasted_iota(jnp.int32, (16, STATE), 1)
    for b in range(rows):
        hit = (lane == b) | (lane == rows + b) | (lane == 2 * rows + b) | (lane == 3 * rows + b)
        pick[b] = jnp.where(hit, 1.0, 0.0).astype(jnp.bfloat16)

    row = lax.broadcasted_iota(jnp.int32, (2 * rows, STATE), 0)
    lane = lax.broadcasted_iota(jnp.int32, (2 * rows, STATE), 1)
    seq = jnp.where(row >= rows, row - rows, row)
    owner = jnp.where((row >= rows) == (lane >= HEAD_DIM), seq, -1)

    def copy_out(i):
        at = pl.ds(2 * i, 2)
        return pltpu.make_async_copy(fresh.at[:, at], state_out.at[:, at], out_sem.at[i])

    def one_pair(i):
        maps = maps_act[:, pl.ds(pl.multiple_of(i * wide, wide), wide)].astype(jnp.float32)
        ins = []
        for hh in range(2):
            ins += [maps[:, 2 * hh * STATE : (2 * hh + 1) * STATE]] * 2
        blank = jnp.zeros((2 * rows, STATE), jnp.float32)
        none = jnp.zeros((STATE - 4 * rows, STATE), jnp.float32)
        left = jnp.concatenate(ins[:2] + [blank, none], axis=0)
        right = jnp.concatenate([blank] + ins[2:] + [none], axis=0)
        into = jnp.concatenate([left, right], axis=1).astype(jnp.bfloat16)
        readers = jnp.concatenate(
            [maps[:, STATE : 2 * STATE], maps[:, 3 * STATE :]], axis=0
        ).astype(jnp.bfloat16)
        values = spread[i]
        found_all = jnp.zeros((2 * rows, pair), jnp.float32)
        for b in range(0, rows, group):
            count = min(group, rows - b)
            chosen = jnp.concatenate(
                [values * jnp.concatenate([pick[b + k]] * (HEAD_DIM // 16), axis=0) for k in range(count)],
                axis=0,
            )
            written = jnp.dot(chosen, into, preferred_element_type=jnp.float32)
            for k0 in range(0, count, 2):
                news = []
                for k in range(k0, k0 + 2):
                    for hh in range(2):
                        h = 2 * i + hh
                        new = (
                            decay[h, pl.ds(b + k, 1), :] * state[b + k, h]
                            + written[
                                k * HEAD_DIM : (k + 1) * HEAD_DIM, hh * STATE : (hh + 1) * STATE
                            ]
                        )
                        fresh[b + k, h] = new
                        news.append(new.astype(jnp.bfloat16))
                found = lax.dot_general(
                    readers,
                    jnp.concatenate(news, axis=0),
                    NT,
                    preferred_element_type=jnp.float32,
                )
                for k in range(2):
                    found_all = found_all + jnp.where(
                        owner == b + k0 + k, found[:, k * pair : (k + 1) * pair], 0.0
                    )
        read[:, pl.ds(pl.multiple_of(i * pair, pair), pair)] = found_all[:rows] + found_all[rows:]

        @pl.when(i > 0)
        def _():
            copy_out(i - 1).start(priority=1)

    steps = 2 if (heads // 2) % 2 == 0 else 1

    def body(j, carry):
        for k in range(steps):
            one_pair(j * steps + k)
        return carry

    lax.fori_loop(0, heads // 2 // steps, body, 0)

    loads[0].wait()
    first = lax.broadcasted_iota(jnp.int32, (rows, pair), 1) < HEAD_DIM
    for i in range(heads // 2):
        at = slice(i * pair, (i + 1) * pair)
        gated = (read[:, at] + direct[:, at]) * gate[:, at]
        square = gated * gated
        low = jnp.sum(jnp.where(first, square, 0.0), axis=1, keepdims=True)
        top = jnp.sum(jnp.where(first, 0.0, square), axis=1, keepdims=True)
        inv = lax.rsqrt(jnp.where(first, low, top) / HEAD_DIM + NORM_EPS)
        heads_out[:, at] = (gated * inv * head_gain[:, at]).astype(jnp.bfloat16)
    copy_out(heads // 2 - 1).start(priority=1)
    loads[1].wait()
    for cp in tails:
        cp.wait()
    for i in range(heads // 2):
        copy_out(i).wait()


def step_state(parts, head_gain, w_out):
    state, past_v, past_m = parts[9], parts[7], parts[8]
    rows, heads = state.shape[:2]
    f32, bf16 = jnp.float32, jnp.bfloat16
    vmem = pl.BlockSpec(memory_space=pltpu.VMEM)
    hbm = pl.BlockSpec(memory_space=pl.ANY)
    return pl.pallas_call(
        state_kernel,
        out_shape=(
            pltpu.VMEM((rows, heads * HEAD_DIM), bf16),
            pltpu.VMEM(w_out.shape, bf16),
            pltpu.HBM(state.shape, f32),
            pltpu.HBM(past_v.shape, bf16),
            pltpu.HBM(past_m.shape, bf16),
        ),
        in_specs=[vmem] * 10 + [hbm] * 2,
        out_specs=(vmem, vmem, hbm, hbm, hbm),
        scratch_shapes=[
            pltpu.VMEM(state.shape, f32),
            pltpu.VMEM((rows, 16, STATE), bf16),
            pltpu.VMEM((rows, heads * HEAD_DIM), f32),
            pltpu.VMEM((1, heads * HEAD_DIM), f32),
            pltpu.SemaphoreType.DMA((2,)),
            pltpu.SemaphoreType.DMA((2, 2)),
            pltpu.SemaphoreType.DMA((heads // 2,)),
        ],
        compiler_params=pltpu.CompilerParams(vmem_limit_bytes=16 * 1024 * 1024),
        name="step_state",
    )(*in_vmem(*parts), *in_hbm(head_gain[None, :], w_out))


def mixer_kernel(
    peers,
    heads,
    out_w,
    tokens_in,
    gain_in,
    w_up,
    w_down,
    layer_out,
    tokens,
    gain,
    up_w,
    down_w,
    sums_a,
    land_a,
    own_hidden,
    hidden,
    squared,
    sums_b,
    land_b,
    small_sem,
    up_sem,
    down_sem,
    send_a,
    recv_a,
    send_h,
    recv_h,
    send_b,
    recv_b,
):
    me = lax.axis_index("kv")
    rows, part = tokens.shape

    def place(d):
        return pl.multiple_of(partner(me, d) * part, part)

    order = far_first(peers) + [0]
    greet(peers, me)
    small = [
        pltpu.make_async_copy(tokens_in, tokens, small_sem.at[0]),
        pltpu.make_async_copy(gain_in, gain, small_sem.at[1]),
    ]
    ups = [
        pltpu.make_async_copy(w_up.at[pl.ds(place(d), part), :], up_w.at[d], up_sem.at[d])
        for d in range(peers)
    ]
    downs = [
        pltpu.make_async_copy(w_down.at[:, pl.ds(place(d), part)], down_w.at[d], down_sem.at[d])
        for d in range(peers)
    ]
    for cp in small:
        cp.start()

    pending = []

    def scatter(left, weights, sums, land, send, recv, after=None):
        for d in order:
            piece = jnp.dot(left, weights(d), preferred_element_type=jnp.float32)
            if d == 0:
                total = piece
            else:
                sums[d] = piece.astype(jnp.bfloat16)
                if not pending:
                    all_here(peers)
                cp = push(sums.at[d], land.at[d], send.at[d], recv.at[d], partner(me, d))
                cp.start()
                pending.append(cp)
        if after is not None:
            after()
        for d in range(1, peers):
            push(sums.at[d], land.at[d], send.at[d], recv.at[d], me).wait_recv()
            total = total + land[d].astype(jnp.float32)
        return total

    def out_block(d):
        return out_w[:, pl.ds(place(d), part)]

    def down_block(d):
        downs[d].wait()
        return down_w[d]

    def load_later():
        for cp in ups:
            cp.start(priority=1)
        for d in order:
            downs[d].start(priority=1)

    total = scatter(heads[...], out_block, sums_a, land_a, send_a, recv_a, load_later)
    for cp in small:
        cp.wait()
    mine = (tokens[...].astype(jnp.float32) + total).astype(jnp.bfloat16)
    own_hidden[...] = mine
    for d in far_first(peers):
        cp = push(own_hidden, hidden.at[d], send_h.at[d], recv_h.at[d], partner(me, d))
        cp.start()
        pending.append(cp)

    squares = jnp.zeros((rows, 1), jnp.float32)
    up = None
    for d in range(peers):
        if d == 0:
            raw = mine
        else:
            push(own_hidden, hidden.at[d], send_h.at[d], recv_h.at[d], me).wait_recv()
            raw = hidden[d]
        wide = raw.astype(jnp.float32)
        squares = squares + jnp.sum(wide * wide, axis=1, keepdims=True)
        scaled = jnp.concatenate(split(wide * gain[:, pl.ds(place(d), part)]), axis=0)
        ups[d].wait()
        out = jnp.dot(
            scaled.astype(jnp.bfloat16), up_w[d], preferred_element_type=jnp.float32
        )
        out = out[:rows] + out[rows:]
        up = out if d == 0 else up + out

    inv = lax.rsqrt(squares / (peers * part) + NORM_EPS)
    up = jnp.maximum(up * inv, 0.0)
    squared[...] = (up * up).astype(jnp.bfloat16)
    total = scatter(squared[...], down_block, sums_b, land_b, send_b, recv_b)
    layer_out[...] = (mine.astype(jnp.float32) + total).astype(jnp.bfloat16)
    for cp in pending:
        cp.wait_send()


def mix_channels(peers, heads_out, out_w, tokens, mlp_gain, w_up, w_down):
    rows, part = tokens.shape
    inner, hid = out_w.shape[0], w_up.shape[1]
    f32, bf16 = jnp.float32, jnp.bfloat16
    vmem = pl.BlockSpec(memory_space=pltpu.VMEM)
    hbm = pl.BlockSpec(memory_space=pl.ANY)
    sems = pltpu.SemaphoreType.DMA((peers,))
    slots = pltpu.VMEM((peers, rows, part), bf16)
    return pl.pallas_call(
        functools.partial(mixer_kernel, peers),
        out_shape=jax.ShapeDtypeStruct((rows, part), bf16),
        in_specs=[vmem] * 2 + [hbm] * 4,
        out_specs=vmem,
        scratch_shapes=[
            pltpu.VMEM((rows, part), bf16),
            pltpu.VMEM((1, peers * part), f32),
            pltpu.VMEM((peers, part, hid), bf16),
            pltpu.VMEM((peers, hid, part), bf16),
            slots,
            slots,
            pltpu.VMEM((rows, part), bf16),
            slots,
            pltpu.VMEM((rows, hid), bf16),
            slots,
            slots,
            pltpu.SemaphoreType.DMA((2,)),
            sems,
            sems,
            sems,
            sems,
            sems,
            sems,
            sems,
            sems,
        ],
        compiler_params=pltpu.CompilerParams(
            collective_id=1, has_side_effects=True, vmem_limit_bytes=24 * 1024 * 1024
        ),
        name="mix_channels",
    )(*in_vmem(heads_out, out_w), *in_hbm(tokens, mlp_gain[None, :], w_up, w_down))


def local_kernels(
    peers,
    tokens,
    mix_gain,
    w_gate,
    w_value,
    w_maps,
    w_step,
    conv_value,
    conv_maps,
    past_value,
    past_maps,
    step_bias,
    decay_log,
    skip_gain,
    head_gain,
    state,
    w_out,
    mlp_gain,
    w_up,
    w_down,
):
    parts = project(
        peers,
        tokens,
        mix_gain,
        w_step,
        step_bias,
        decay_log,
        skip_gain,
        conv_value,
        conv_maps,
        w_gate,
        w_value,
        w_maps,
        jnp.swapaxes(past_value, 0, 1),
        jnp.swapaxes(past_maps, 0, 1),
        state,
    )
    heads_out, out_w, state_next, tail_v, tail_m = step_state(parts, head_gain, w_out)
    layer_out = mix_channels(peers, heads_out, out_w, tokens, mlp_gain, w_up, w_down)
    return layer_out, state_next, jnp.swapaxes(tail_v, 0, 1), jnp.swapaxes(tail_m, 0, 1)


def kernels_fit(peers, tokens, state, w_maps, w_up):
    rows, part = tokens.shape
    heads = state.shape[1]
    inner = heads * HEAD_DIM
    weights = 2 * tokens.shape[1] * peers * (2 * inner + w_maps.shape[1])
    held = 4 * rows * heads * HEAD_DIM * STATE
    later = 2 * part * peers * (inner + 2 * w_up.shape[1])
    mib = 1024 * 1024
    return (
        peers > 1
        and peers & (peers - 1) == 0
        and rows % 8 == 0
        and 4 * rows <= STATE
        and part % 128 == 0
        and heads % 2 == 0
        and w_maps.shape[1] == heads * 2 * STATE
        and w_up.shape[1] % 128 == 0
        and weights + held <= 40 * mib
        and 2 * held + 2 * part * peers * inner <= 40 * mib
        and later <= 40 * mib
    )


def rms_rows(matrix, gain_vec):
    widened = matrix.astype(jnp.float32)
    inv_scale = lax.rsqrt(jnp.mean(widened * widened, axis=-1, keepdims=True) + NORM_EPS)
    return (widened * inv_scale * gain_vec).astype(jnp.bfloat16)


def short_conv(past_rows, newest, kernel):
    window = jnp.concatenate([past_rows, newest[:, None, :]], axis=1)
    summed = jnp.sum(window.astype(jnp.float32) * kernel[None], axis=1)
    return (jax.nn.silu(summed), window[:, 1:, :])


def local(
    tokens,
    mix_gain,
    w_gate,
    w_value,
    w_maps,
    w_step,
    conv_value,
    conv_maps,
    past_value,
    past_maps,
    step_bias,
    decay_log,
    skip_gain,
    head_gain,
    state,
    w_out,
    mlp_gain,
    w_up,
    w_down,
):
    whole_rows = lax.all_gather(tokens, "kv", axis=1, tiled=True)
    batch_rows = whole_rows.shape[0]
    heads_here = state.shape[1]
    head_start = lax.axis_index("kv") * heads_here
    normed = rms_rows(whole_rows, mix_gain)
    gate_pre = jnp.dot(normed, w_gate, preferred_element_type=jnp.float32)
    step_cols = lax.dynamic_slice_in_dim(w_step, head_start, heads_here, 1)
    step_pre = jnp.dot(normed, step_cols, preferred_element_type=jnp.float32)
    value_new = jnp.dot(normed, w_value, preferred_element_type=jnp.float32).astype(jnp.bfloat16)
    maps_new = jnp.dot(normed, w_maps, preferred_element_type=jnp.float32).astype(jnp.bfloat16)
    value_act, value_tail = short_conv(past_value, value_new, conv_value)
    maps_act, maps_tail = short_conv(past_maps, maps_new, conv_maps)
    maps_act = lax.optimization_barrier(maps_act.astype(jnp.bfloat16))
    grouped = maps_act.astype(jnp.float32).reshape(batch_rows, -1, 2, STATE)
    per_group = heads_here // grouped.shape[1]
    in_map = jnp.repeat(grouped[:, :, 0], per_group, axis=1)
    out_map = jnp.repeat(grouped[:, :, 1], per_group, axis=1)
    head_values = value_act.reshape(batch_rows, heads_here, HEAD_DIM)
    step_size = jax.nn.softplus(step_pre + step_bias)
    decay_rate = jnp.exp(-step_size * jnp.exp(decay_log))
    written = (step_size[:, :, None] * head_values)[:, :, :, None] * in_map[:, :, None, :]
    state_next = decay_rate[:, :, None, None] * state + written
    read_out = (
        jnp.sum(state_next * out_map[:, :, None, :], axis=-1)
        + skip_gain[None, :, None] * head_values
    )
    gated_heads = read_out * jax.nn.silu(gate_pre.reshape(batch_rows, heads_here, HEAD_DIM))
    inv_scale = lax.rsqrt(jnp.mean(gated_heads * gated_heads, axis=-1, keepdims=True) + NORM_EPS)
    heads_out = gated_heads * inv_scale * head_gain.reshape(heads_here, HEAD_DIM)
    heads_out = heads_out.reshape(batch_rows, heads_here * HEAD_DIM).astype(jnp.bfloat16)
    partial_value = jnp.dot(heads_out, w_out, preferred_element_type=jnp.float32)
    own_part = lax.psum_scatter(partial_value, "kv", scatter_dimension=1, tiled=True)
    own_hidden = lax.optimization_barrier(
        (tokens.astype(jnp.float32) + own_part).astype(jnp.bfloat16)
    )
    hidden = lax.all_gather(own_hidden, "kv", axis=1, tiled=True)
    normed_mlp = rms_rows(hidden, mlp_gain)
    squared = jnp.square(jax.nn.relu(jnp.dot(normed_mlp, w_up, preferred_element_type=jnp.float32)))
    squared = squared.astype(jnp.bfloat16)
    partial_mlp = jnp.dot(squared, w_down, preferred_element_type=jnp.float32)
    mlp_part = lax.psum_scatter(partial_mlp, "kv", scatter_dimension=1, tiled=True)
    layer_out = (own_hidden.astype(jnp.float32) + mlp_part).astype(jnp.bfloat16)
    return (layer_out, state_next, value_tail, maps_tail)


def solution(mesh):
    in_specs = (
        P(("dp", "tp"), "kv"),
        P(),
        P(None, "kv"),
        P(None, "kv"),
        P(None, "kv"),
        P(),
        P(None, "kv"),
        P(None, "kv"),
        P(("dp", "tp"), None, "kv"),
        P(("dp", "tp"), None, "kv"),
        P("kv"),
        P("kv"),
        P("kv"),
        P("kv"),
        P(("dp", "tp"), "kv", None, None),
        P("kv", None),
        P(),
        P(None, "kv"),
        P("kv", None),
    )
    out_specs = (
        P(("dp", "tp"), "kv"),
        P(("dp", "tp"), "kv", None, None),
        P(("dp", "tp"), None, "kv"),
        P(("dp", "tp"), None, "kv"),
    )
    peers = mesh.shape["kv"]

    def device_part(*args):
        if kernels_fit(peers, args[0], args[14], args[4], args[17]):
            return local_kernels(peers, *args)
        return local(*args)

    return jax.shard_map(
        device_part, mesh=mesh, in_specs=in_specs, out_specs=out_specs, check_vma=False
    )
```

time: 52.6 us -> 39.9 us (0.76)
  Pallas kernels: 50.3 us -> 38.5 us
  local copies, waits for them, and re-layouts: 1.35 us -> 0.61 us
    pallas_call x2, Pallas kernels: 29.4 us -> 22.2 us  [the longest x1 15.9 us: project(): pl.pallas_call(functools.partial(project_kernel, peers), out_shape=(pltpu...]
    pallas_call x1, Pallas kernels: 20.9 us -> 16.3 us  [mix_channels(): pl.pallas_call(functools.partial(mixer_kernel, peers), out_shape=jax.Shap...]
    unnamed x1, local copies, waits for them, and re-layouts: 1.35 us -> 0.61 us
where the time goes in v1:
time: 39.9 us; the launch traced here: 39.7 us
  Pallas kernels  38.5 us (96%)
  between operations  0.66 us (2%)
  local copies, waits for them, and re-layouts  0.61 us (2%)
    pallas_call x1, Pallas kernels, mix_channels(): pl.pallas_call(functools.partial(mixer_kernel, peers), out_shape=jax.Shap...  16.3 us
    pallas_call x1, Pallas kernels, project(): pl.pallas_call(functools.partial(project_kernel, peers), out_shape=(pltpu...  15.9 us
    pallas_call x1, Pallas kernels, step_state(): pl.pallas_call(state_kernel, out_shape=(pltpu.VMEM((rows, heads * HEAD_DI...  6.31 us

profile of v1, /device:TPU:0, one launch (start us, length us, event | category | flops | bytes accessed | tf_op | source)
XLA Modules:
  0.0 39.7 jit_solution(15801452650559900861)
XLA Ops:
  0.6 15.9 %project.1 = (f32[24,1024]{1,0:T(8,128)S(1)}, f32[24,1024]{1,0:T(8,128)S(1)}, bf16[24,1024]{1,0:T(8,128)(2,1)S(1)}, bf16[24,4096]{1,0:T(8,128)(2,1)S(1)}, bf16[2...) custom-call(bf16[24,512]{1,0:T(8,128)(2,1)} %tokens_in.3, ...), custom_call_target="tpu_custom_call" | custom-call | tf_op jit(solution)/shard_map/project/pallas_call | solution.py:292
  16.5 6.3 %step_state.1 = (bf16[24,1024]{1,0:T(8,128)(2,1)S(1)}, bf16[1024,2048]{1,0:T(8,128)(2,1)S(1)}, f32[24,16,64,128]{3,2,1,0:T(8,128)}, bf16[3,24,1024]{2,1,0:T(8,128)(2,1)}, bf16[3,24,4096]{2,1,0:T(8,128)(2,1)}) custom-call(f32[24,1024]{1,0:T(8,128)S(1)} %get-tuple-element.19.gate, f32[24,1024]{1,0:T(8,128)S(1)} %get-tuple-element.20.direct, ...), custom_call_target="tpu_custom_call" | custom-call | tf_op jit(solution)/shard_map/step_state/pallas_call | solution.py:496
  22.9 16.3 %mix_channels.1 = bf16[24,512]{1,0:T(8,128)(2,1)S(1)} custom-call(bf16[24,1024]{1,0:T(8,128)(2,1)S(1)} %get-tuple-element.29.heads, bf16[1024,2048]{1,0:T(8,128)(2,1)S(1)} %get-tuple-element.30.out_w, bf16[24,512]{1,0:T(8,128)(2,1)} %tokens_in.3, f32[1,2048]{1,0:T(1,128)} %bitcast.15, bf16[2048,2048]{1,0:T(8,128)(2,1)} %w_up.1, bf16[2048,2048]{1,0:T(8,128)(2,1)} %w_down.1), custom_call_target="tpu_custom_call" | custom-call | tf_op jit(solution)/shard_map/mix_channels/pallas_call | solution.py:653
  39.1 0.6 %copy.24 = bf16[24,512]{1,0:T(8,128)(2,1)} copy(bf16[24,512]{1,0:T(8,128)(2,1)S(1)} %mix_channels.1) | data formatting | bytes 49152

commit v2 on v1

v2 whole, which is shorter than its diff:
```python
import functools

import jax
import jax.numpy as jnp
from jax import lax
from jax.experimental import pallas as pl
from jax.experimental.pallas import tpu as pltpu
from jax.sharding import PartitionSpec as P

HEAD_DIM = 64
STATE = 128
MESH = pl.DeviceIdType.MESH
FUSED_LIMIT = 49 * 1024 * 1024
WINDOW = 9


NORM_EPS = 1e-05
NT = (((1,), (1,)), ((), ()))


def partner(me, d):
    other = me
    bit = 1
    while bit <= d:
        if d & bit:
            other = other + bit - 2 * bit * lax.rem(lax.div(me, bit), 2)
        bit *= 2
    return other


def greet(peers, me):
    for d in range(1, peers):
        pl.semaphore_signal(
            pltpu.get_barrier_semaphore(),
            inc=1,
            device_id={"kv": partner(me, d)},
            device_id_type=MESH,
        )


def all_here(peers):
    pl.semaphore_wait(pltpu.get_barrier_semaphore(), peers - 1)


def far_first(peers):
    return list(range(1, peers))[::-1]


def push(src, dst, send_sem, recv_sem, target):
    return pltpu.make_async_remote_copy(
        src_ref=src,
        dst_ref=dst,
        send_sem=send_sem,
        recv_sem=recv_sem,
        device_id={"kv": target},
        device_id_type=MESH,
    )


def in_hbm(*arrays):
    return [pltpu.with_memory_space_constraint(x, pltpu.HBM) for x in arrays]


def in_vmem(*arrays):
    return [pltpu.with_memory_space_constraint(x, pltpu.VMEM) for x in arrays]


def silu(x):
    return x * jax.nn.sigmoid(x)


def split(x):
    high = x.astype(jnp.bfloat16).astype(jnp.float32)
    return high, x - high


def decode_kernel(
    peers,
    tokens_in,
    gain_in,
    w_step_in,
    bias_in,
    decay_log_in,
    skip_in,
    head_gain_in,
    mlp_gain_in,
    conv_value_in,
    conv_maps_in,
    past_value_in,
    past_maps_in,
    w_gate,
    w_value,
    w_maps,
    state_in,
    w_out,
    w_up,
    w_down,
    layer_out,
    value_new,
    maps_new,
    past_value,
    past_maps,
    state,
    tokens,
    gain,
    w_step,
    bias,
    decay_log,
    skip,
    head_gain,
    mlp_gain,
    conv_value,
    conv_maps,
    slots,
    weights,
    acc,
    gate,
    value_act,
    maps_act,
    decay_rows,
    step_cols,
    spread,
    pick,
    readers,
    read,
    out_w,
    up_w,
    down_w,
    sums_a,
    land_a,
    own_hidden,
    hidden,
    squared,
    sums_b,
    land_b,
    small_sem,
    w_sem,
    state_sem,
    out_sem,
    up_sem,
    down_sem,
    send_t,
    recv_t,
    send_a,
    recv_a,
    send_h,
    recv_h,
    send_b,
    recv_b,
):
    me = lax.axis_index("kv")
    rows, part = tokens.shape
    chunks, width = weights.shape[1], weights.shape[3]
    heads = bias.shape[1]
    inner = value_new.shape[1]
    pair = 2 * HEAD_DIM
    wide = 4 * STATE
    taps = past_value.shape[0]
    pairs = heads // 2
    greet(peers, me)

    def place(d):
        return pl.multiple_of(partner(me, d) * part, part)

    small = [
        pltpu.make_async_copy(src, dst, small_sem.at[k])
        for k, (src, dst) in enumerate(
            (
                (tokens_in, tokens),
                (gain_in, gain),
                (w_step_in, w_step),
                (bias_in, bias),
                (decay_log_in, decay_log),
                (skip_in, skip),
                (head_gain_in, head_gain),
                (mlp_gain_in, mlp_gain),
                (conv_value_in, conv_value),
                (conv_maps_in, conv_maps),
                (past_value_in, past_value),
                (past_maps_in, past_maps),
            )
        )
    ]

    def weight_copies(d, c):
        if c == 0:
            return [
                pltpu.make_async_copy(
                    ref.at[pl.ds(place(d), part), :],
                    weights.at[d, 0, :, pl.ds(k * inner, inner)],
                    w_sem.at[d, 0],
                )
                for k, ref in enumerate((w_gate, w_value))
            ]
        return [
            pltpu.make_async_copy(
                w_maps.at[pl.ds(place(d), part), pl.ds((c - 1) * width, width)],
                weights.at[d, c],
                w_sem.at[d, c],
            )
        ]

    blocks = state_sem.shape[0]
    block = rows // blocks

    def state_copy(r):
        at = pl.ds(r * block, block)
        return pltpu.make_async_copy(state_in.at[at], state.at[at], state_sem.at[r])

    order = far_first(peers) + [0]
    outs = [
        pltpu.make_async_copy(w_out.at[:, pl.ds(place(d), part)], out_w.at[d], out_sem.at[d])
        for d in range(peers)
    ]
    ups = [
        pltpu.make_async_copy(w_up.at[pl.ds(place(d), part), :], up_w.at[d], up_sem.at[d])
        for d in range(peers)
    ]
    downs = [
        pltpu.make_async_copy(w_down.at[:, pl.ds(place(d), part)], down_w.at[d], down_sem.at[d])
        for d in range(peers)
    ]
    bulk = [weight_copies(d, c) for d in range(peers) for c in range(chunks)]
    bulk += [[state_copy(r)] for r in range(blocks)] + [[outs[d]] for d in order]

    def load(count):
        for _ in range(min(count, len(bulk))):
            for cp in bulk.pop(0):
                cp.start(priority=1)

    for cp in small[:3]:
        cp.start()
    load(chunks)
    small[0].wait()
    all_here(peers)
    pending = []

    def send(src, dst, send_sem, recv_sem, d):
        cp = push(src, dst, send_sem.at[d], recv_sem.at[d], partner(me, d))
        cp.start()
        pending.append(cp)

    def arrived(src, dst, send_sem, recv_sem, d):
        push(src, dst, send_sem.at[d], recv_sem.at[d], me).wait_recv()

    for d in far_first(peers):
        send(tokens, slots.at[d], send_t, recv_t, d)
    for cp in small[3:]:
        cp.start()
    load(WINDOW - chunks)
    for cp in small[1:]:
        cp.wait()

    lane = lax.broadcasted_iota(jnp.int32, (rows, pair), 1)

    def by_head(table, h):
        return jnp.where(lane < HEAD_DIM, table[:, h : h + 1], table[:, h + 1 : h + 2])

    squares = jnp.zeros((rows, 1), jnp.float32)
    step_pre = jnp.zeros((2 * rows, w_step.shape[0]), jnp.float32)
    for d in range(peers):
        if d == 0:
            raw = tokens[...]
        else:
            arrived(tokens, slots.at[d], send_t, recv_t, d)
            raw = slots[d]
        x = raw.astype(jnp.float32)
        squares = squares + jnp.sum(x * x, axis=1, keepdims=True)
        scaled = jnp.concatenate(split(x * gain[:, pl.ds(place(d), part)]), axis=0)
        scaled = scaled.astype(jnp.bfloat16)
        step_pre = step_pre + lax.dot_general(
            scaled, w_step[:, pl.ds(place(d), part)], NT, preferred_element_type=jnp.float32
        )
        last = d == peers - 1
        if last:
            inv = lax.rsqrt(squares / (peers * part) + NORM_EPS)
            step_pre = (step_pre[:rows] + step_pre[rows:]) * inv
            own = step_pre[:, :heads]
            for j in range(1, peers):
                own = jnp.where(me == j, step_pre[:, j * heads : (j + 1) * heads], own)
            own = own + bias[...]
            step = jnp.maximum(own, 0.0) + jnp.log1p(jnp.exp(-jnp.abs(own)))
            decay = jnp.exp(-step * jnp.exp(decay_log[...]))
            for h in range(heads):
                decay_rows[h] = jnp.broadcast_to(decay[:, h : h + 1], (rows, STATE))
            for h in range(0, heads, 2):
                step_cols[:, h * HEAD_DIM : (h + 2) * HEAD_DIM] = by_head(step, h)

        for c in range(chunks):
            pltpu.make_async_copy(
                w_maps.at[pl.ds(0, part), pl.ds(0, width)], weights.at[d, c], w_sem.at[d, c]
            ).wait()
            load(1)
            out = jnp.dot(scaled, weights[d, c], preferred_element_type=jnp.float32)
            out = out[:rows] + out[rows:]
            total = out if d == 0 else acc[c] + out
            if not last:
                acc[c] = total
                continue
            total = total * inv

            def conv(new, past, at, cols, table):
                summed = new.astype(jnp.float32) * table[taps : taps + 1, at : at + cols]
                for k in range(taps):
                    row = past[k, :, at : at + cols].astype(jnp.float32)
                    summed = summed + row * table[k : k + 1, at : at + cols]
                return silu(summed)

            if c == 0:
                gate[...] = silu(total[:, :inner])
                new = total[:, inner:].astype(jnp.bfloat16)
                value_new[...] = new
                value_act[...] = conv(new, past_value, 0, inner, conv_value)
            else:
                at = (c - 1) * width
                new = total.astype(jnp.bfloat16)
                maps_new[:, at : at + width] = new
                act = conv(new, past_maps, at, width, conv_maps)
                maps_act[:, at : at + width] = act.astype(jnp.bfloat16)

    row = lax.broadcasted_iota(jnp.int32, (2 * rows, STATE), 0)
    column = lax.broadcasted_iota(jnp.int32, (2 * rows, STATE), 1)
    seq = jnp.where(row >= rows, row - rows, row)
    owner = jnp.where((row >= rows) == (column >= HEAD_DIM), seq, -1)
    read[...] = jnp.zeros_like(read)

    for i in range(pairs):
        at = i * wide
        readers[i] = jnp.concatenate(
            [
                maps_act[:, at + STATE : at + 2 * STATE].astype(jnp.float32),
                maps_act[:, at + 3 * STATE : at + wide].astype(jnp.float32),
            ],
            axis=0,
        ).astype(jnp.bfloat16)

    def read_pair(i, r):
        total = read[i]
        for k0 in range(0, block, 2):
            tiles = []
            for k in range(k0, k0 + 2):
                for hh in range(2):
                    tiles.append(state[r * block + k, 2 * i + hh].astype(jnp.bfloat16))
            found = lax.dot_general(
                readers[i], jnp.concatenate(tiles, axis=0), NT, preferred_element_type=jnp.float32
            )
            for k in range(2):
                total = total + jnp.where(
                    owner == r * block + k0 + k, found[:, k * pair : (k + 1) * pair], 0.0
                )
        read[i] = total

    for r in range(blocks):
        state_copy(r).wait()
        load(1)
        for i in range(pairs):
            read_pair(i, r)
    load(len(bulk))

    heads_out = []
    first = lane < HEAD_DIM
    for i in range(pairs):
        at = slice(i * pair, (i + 1) * pair)
        act = value_act[:, at]
        scaled = act * step_cols[:, at]
        inner_dots = []
        for hh in range(2):
            m = i * wide + 2 * hh * STATE
            into = maps_act[:, m : m + STATE].astype(jnp.float32)
            outof = maps_act[:, m + STATE : m + 2 * STATE].astype(jnp.float32)
            inner_dots.append(jnp.sum(into * outof, axis=1, keepdims=True))
        h = 2 * i
        decayed = jnp.where(first, decay_rows[h], decay_rows[h + 1])
        found = read[i]
        read_out = decayed * (found[:rows] + found[rows:])
        read_out = read_out + jnp.where(first, inner_dots[0], inner_dots[1]) * scaled
        gated = (read_out + by_head(skip, h) * act) * gate[:, at]
        square = gated * gated
        low = jnp.sum(jnp.where(first, square, 0.0), axis=1, keepdims=True)
        top = jnp.sum(jnp.where(first, 0.0, square), axis=1, keepdims=True)
        norm = lax.rsqrt(jnp.where(first, low, top) / HEAD_DIM + NORM_EPS)
        heads_out.append((gated * norm * head_gain[:, at]).astype(jnp.bfloat16))
    heads_out = jnp.concatenate(heads_out, axis=1)

    def scatter(left, waits, weight, sums, land, send_sem, recv_sem, between):
        for d in order:
            waits[d].wait()
            piece = jnp.dot(left, weight[d], preferred_element_type=jnp.float32)
            if d == 0:
                total = piece
            else:
                sums[d] = piece.astype(jnp.bfloat16)
                send(sums.at[d], land.at[d], send_sem, recv_sem, d)
        between()
        for d in range(1, peers):
            arrived(sums.at[d], land.at[d], send_sem, recv_sem, d)
            total = total + land[d].astype(jnp.float32)
        return total

    def prepare():
        spot = lax.broadcasted_iota(jnp.int32, (16, STATE), 1)
        for b in range(rows):
            hit = (spot == b) | (spot == rows + b)
            hit = hit | (spot == 2 * rows + b) | (spot == 3 * rows + b)
            pick[b] = jnp.where(hit, 1.0, 0.0).astype(jnp.bfloat16)
        blank = jnp.zeros((STATE - 4 * rows, HEAD_DIM), jnp.float32)
        for i in range(pairs):
            at = slice(i * pair, (i + 1) * pair)
            both = jnp.concatenate(split(value_act[:, at] * step_cols[:, at]), axis=0)
            stack = jnp.concatenate([both[:, :HEAD_DIM], both[:, HEAD_DIM:], blank], axis=0)
            spread[i] = stack.T.astype(jnp.bfloat16)

    def update(i, carry):
        maps = maps_act[:, pl.ds(pl.multiple_of(i * wide, wide), wide)].astype(jnp.float32)
        ins = []
        for hh in range(2):
            ins += [maps[:, 2 * hh * STATE : (2 * hh + 1) * STATE]] * 2
        blank = jnp.zeros((2 * rows, STATE), jnp.float32)
        none = jnp.zeros((STATE - 4 * rows, STATE), jnp.float32)
        left = jnp.concatenate(ins[:2] + [blank, none], axis=0)
        right = jnp.concatenate([blank] + ins[2:] + [none], axis=0)
        into = jnp.concatenate([left, right], axis=1).astype(jnp.bfloat16)
        values = spread[i]
        for b in range(0, rows, 4):
            chosen = jnp.concatenate(
                [
                    values * jnp.concatenate([pick[b + k]] * (HEAD_DIM // 16), axis=0)
                    for k in range(4)
                ],
                axis=0,
            )
            written = jnp.dot(chosen, into, preferred_element_type=jnp.float32)
            for k in range(4):
                for hh in range(2):
                    h = 2 * i + hh
                    state[b + k, h] = (
                        decay_rows[h, pl.ds(b + k, 1), :] * state[b + k, h]
                        + written[k * HEAD_DIM : (k + 1) * HEAD_DIM, hh * STATE : (hh + 1) * STATE]
                    )
        return carry

    def first_half():
        for cp in ups:
            cp.start(priority=1)
        prepare()
        lax.fori_loop(0, pairs // 2, update, 0)

    total = scatter(heads_out, outs, out_w, sums_a, land_a, send_a, recv_a, first_half)
    mine = (tokens[...].astype(jnp.float32) + total).astype(jnp.bfloat16)
    own_hidden[...] = mine
    for d in far_first(peers):
        send(own_hidden, hidden.at[d], send_h, recv_h, d)
    for d in order:
        downs[d].start(priority=1)
    lax.fori_loop(pairs // 2, pairs, update, 0)

    squares = jnp.zeros((rows, 1), jnp.float32)
    for d in range(peers):
        if d == 0:
            raw = mine
        else:
            arrived(own_hidden, hidden.at[d], send_h, recv_h, d)
            raw = hidden[d]
        x = raw.astype(jnp.float32)
        squares = squares + jnp.sum(x * x, axis=1, keepdims=True)
        scaled = jnp.concatenate(split(x * mlp_gain[:, pl.ds(place(d), part)]), axis=0)
        ups[d].wait()
        out = jnp.dot(scaled.astype(jnp.bfloat16), up_w[d], preferred_element_type=jnp.float32)
        out = out[:rows] + out[rows:]
        up = out if d == 0 else up + out

    inv = lax.rsqrt(squares / (peers * part) + NORM_EPS)
    up = jnp.maximum(up * inv, 0.0)
    squared[...] = (up * up).astype(jnp.bfloat16)
    total = scatter(
        squared[...], downs, down_w, sums_b, land_b, send_b, recv_b, lambda: None
    )
    layer_out[...] = (mine.astype(jnp.float32) + total).astype(jnp.bfloat16)
    for cp in pending:
        cp.wait_send()


def decode(peers, tokens, small, past_value, past_maps, weights, state, later):
    rows, part = tokens.shape
    heads = state.shape[1]
    inner, maps = heads * HEAD_DIM, 2 * heads * STATE
    hid = later[1].shape[1]
    width = 2 * inner
    chunks = 1 + maps // width
    f32, bf16 = jnp.float32, jnp.bfloat16
    block = 4 if rows % 4 == 0 else 2
    vmem = pl.BlockSpec(memory_space=pltpu.VMEM)
    hbm = pl.BlockSpec(memory_space=pl.ANY)
    sems = pltpu.SemaphoreType.DMA((peers,))
    slots = pltpu.VMEM((peers, rows, part), bf16)
    operands = (tokens, *small, past_value, past_maps, *weights, state, *later)
    return pl.pallas_call(
        functools.partial(decode_kernel, peers),
        out_shape=(
            pltpu.VMEM((rows, part), bf16),
            pltpu.VMEM((rows, inner), bf16),
            pltpu.VMEM((rows, maps), bf16),
            pltpu.VMEM(past_value.shape, bf16),
            pltpu.VMEM(past_maps.shape, bf16),
            pltpu.VMEM(state.shape, f32),
        ),
        in_specs=[hbm] * len(operands),
        out_specs=(vmem,) * 6,
        scratch_shapes=[
            pltpu.VMEM((rows, part), bf16),
            *[pltpu.VMEM(x.shape, x.dtype) for x in small],
            slots,
            pltpu.VMEM((peers, chunks, part, width), bf16),
            pltpu.VMEM((chunks, rows, width), f32),
            pltpu.VMEM((rows, inner), f32),
            pltpu.VMEM((rows, inner), f32),
            pltpu.VMEM((rows, maps), bf16),
            pltpu.VMEM((heads, rows, STATE), f32),
            pltpu.VMEM((rows, inner), f32),
            pltpu.VMEM((heads // 2, HEAD_DIM, STATE), bf16),
            pltpu.VMEM((rows, 16, STATE), bf16),
            pltpu.VMEM((heads // 2, 2 * rows, STATE), bf16),
            pltpu.VMEM((heads // 2, 2 * rows, STATE), f32),
            pltpu.VMEM((peers, inner, part), bf16),
            pltpu.VMEM((peers, part, hid), bf16),
            pltpu.VMEM((peers, hid, part), bf16),
            slots,
            slots,
            pltpu.VMEM((rows, part), bf16),
            slots,
            pltpu.VMEM((rows, hid), bf16),
            slots,
            slots,
            pltpu.SemaphoreType.DMA((12,)),
            pltpu.SemaphoreType.DMA((peers, chunks)),
            pltpu.SemaphoreType.DMA((rows // block,)),
            *[sems] * 11,
        ],
        compiler_params=pltpu.CompilerParams(
            collective_id=0, has_side_effects=True, vmem_limit_bytes=FUSED_LIMIT
        ),
        name="decode",
    )(*in_hbm(*operands))


def flush_kernel(
    layer,
    value_new,
    maps_new,
    past_value,
    past_maps,
    state,
    layer_out,
    state_out,
    value_tail,
    maps_tail,
    sem,
    state_sem,
):
    taps = past_value.shape[0]
    blocks = state_sem.shape[0]
    block = state.shape[0] // blocks
    copies = []
    for k in range(blocks):
        at = pl.ds(k * block, block)
        copies.append(pltpu.make_async_copy(state.at[at], state_out.at[at], state_sem.at[k]))
    for k, (past, new, tail) in enumerate(
        ((past_value, value_new, value_tail), (past_maps, maps_new, maps_tail))
    ):
        keep = past.at[pl.ds(1, taps - 1)]
        copies.append(
            pltpu.make_async_copy(keep, tail.at[pl.ds(0, taps - 1)], sem.at[2 * k])
        )
        copies.append(pltpu.make_async_copy(new, tail.at[taps - 1], sem.at[2 * k + 1]))
    copies.append(pltpu.make_async_copy(layer, layer_out, sem.at[4]))
    for cp in copies:
        cp.start(priority=1)
    for cp in copies:
        cp.wait()


def flush(parts):
    layer, _, _, past_v, past_m, state = parts
    f32, bf16 = jnp.float32, jnp.bfloat16
    vmem = pl.BlockSpec(memory_space=pltpu.VMEM)
    hbm = pl.BlockSpec(memory_space=pl.ANY)
    rows = state.shape[0]
    return pl.pallas_call(
        flush_kernel,
        out_shape=(
            pltpu.HBM(layer.shape, bf16),
            pltpu.HBM(state.shape, f32),
            pltpu.HBM(past_v.shape, bf16),
            pltpu.HBM(past_m.shape, bf16),
        ),
        in_specs=[vmem] * 6,
        out_specs=(hbm,) * 4,
        scratch_shapes=[
            pltpu.SemaphoreType.DMA((5,)),
            pltpu.SemaphoreType.DMA((8 if rows % 8 == 0 else 1,)),
        ],
        compiler_params=pltpu.CompilerParams(vmem_limit_bytes=4 * 1024 * 1024),
        name="flush",
    )(*in_vmem(*parts))


def local_kernels(
    peers,
    tokens,
    mix_gain,
    w_gate,
    w_value,
    w_maps,
    w_step,
    conv_value,
    conv_maps,
    past_value,
    past_maps,
    step_bias,
    decay_log,
    skip_gain,
    head_gain,
    state,
    w_out,
    mlp_gain,
    w_up,
    w_down,
):
    small = (
        mix_gain[None, :],
        w_step.T,
        step_bias[None, :],
        decay_log[None, :],
        skip_gain[None, :],
        head_gain[None, :],
        mlp_gain[None, :],
        conv_value,
        conv_maps,
    )
    parts = decode(
        peers,
        tokens,
        small,
        jnp.swapaxes(past_value, 0, 1),
        jnp.swapaxes(past_maps, 0, 1),
        (w_gate, w_value, w_maps),
        state,
        (w_out, w_up, w_down),
    )
    layer_out, state_next, tail_v, tail_m = flush(parts)
    return layer_out, state_next, jnp.swapaxes(tail_v, 0, 1), jnp.swapaxes(tail_m, 0, 1)


def kernels_fit(peers, tokens, state, w_maps, w_up):
    rows, part = tokens.shape
    heads = state.shape[1]
    inner = heads * HEAD_DIM
    weights = 2 * tokens.shape[1] * peers * (2 * inner + w_maps.shape[1])
    later = 2 * part * peers * (inner + 2 * w_up.shape[1])
    held = 4 * rows * heads * HEAD_DIM * STATE
    return (
        peers > 1
        and peers & (peers - 1) == 0
        and rows % 8 == 0
        and 4 * rows <= STATE
        and part % 128 == 0
        and heads % 4 == 0
        and w_maps.shape[1] == heads * 2 * STATE
        and w_up.shape[1] % 128 == 0
        and weights + later <= 44 * 1024 * 1024
        and held <= 12 * 1024 * 1024
    )


def rms_rows(matrix, gain_vec):
    widened = matrix.astype(jnp.float32)
    inv_scale = lax.rsqrt(jnp.mean(widened * widened, axis=-1, keepdims=True) + NORM_EPS)
    return (widened * inv_scale * gain_vec).astype(jnp.bfloat16)


def short_conv(past_rows, newest, kernel):
    window = jnp.concatenate([past_rows, newest[:, None, :]], axis=1)
    summed = jnp.sum(window.astype(jnp.float32) * kernel[None], axis=1)
    return (jax.nn.silu(summed), window[:, 1:, :])


def local(
    tokens,
    mix_gain,
    w_gate,
    w_value,
    w_maps,
    w_step,
    conv_value,
    conv_maps,
    past_value,
    past_maps,
    step_bias,
    decay_log,
    skip_gain,
    head_gain,
    state,
    w_out,
    mlp_gain,
    w_up,
    w_down,
):
    whole_rows = lax.all_gather(tokens, "kv", axis=1, tiled=True)
    batch_rows = whole_rows.shape[0]
    heads_here = state.shape[1]
    head_start = lax.axis_index("kv") * heads_here
    normed = rms_rows(whole_rows, mix_gain)
    gate_pre = jnp.dot(normed, w_gate, preferred_element_type=jnp.float32)
    step_cols = lax.dynamic_slice_in_dim(w_step, head_start, heads_here, 1)
    step_pre = jnp.dot(normed, step_cols, preferred_element_type=jnp.float32)
    value_new = jnp.dot(normed, w_value, preferred_element_type=jnp.float32).astype(jnp.bfloat16)
    maps_new = jnp.dot(normed, w_maps, preferred_element_type=jnp.float32).astype(jnp.bfloat16)
    value_act, value_tail = short_conv(past_value, value_new, conv_value)
    maps_act, maps_tail = short_conv(past_maps, maps_new, conv_maps)
    maps_act = lax.optimization_barrier(maps_act.astype(jnp.bfloat16))
    grouped = maps_act.astype(jnp.float32).reshape(batch_rows, -1, 2, STATE)
    per_group = heads_here // grouped.shape[1]
    in_map = jnp.repeat(grouped[:, :, 0], per_group, axis=1)
    out_map = jnp.repeat(grouped[:, :, 1], per_group, axis=1)
    head_values = value_act.reshape(batch_rows, heads_here, HEAD_DIM)
    step_size = jax.nn.softplus(step_pre + step_bias)
    decay_rate = jnp.exp(-step_size * jnp.exp(decay_log))
    written = (step_size[:, :, None] * head_values)[:, :, :, None] * in_map[:, :, None, :]
    state_next = decay_rate[:, :, None, None] * state + written
    read_out = (
        jnp.sum(state_next * out_map[:, :, None, :], axis=-1)
        + skip_gain[None, :, None] * head_values
    )
    gated_heads = read_out * jax.nn.silu(gate_pre.reshape(batch_rows, heads_here, HEAD_DIM))
    inv_scale = lax.rsqrt(jnp.mean(gated_heads * gated_heads, axis=-1, keepdims=True) + NORM_EPS)
    heads_out = gated_heads * inv_scale * head_gain.reshape(heads_here, HEAD_DIM)
    heads_out = heads_out.reshape(batch_rows, heads_here * HEAD_DIM).astype(jnp.bfloat16)
    partial_value = jnp.dot(heads_out, w_out, preferred_element_type=jnp.float32)
    own_part = lax.psum_scatter(partial_value, "kv", scatter_dimension=1, tiled=True)
    own_hidden = lax.optimization_barrier(
        (tokens.astype(jnp.float32) + own_part).astype(jnp.bfloat16)
    )
    hidden = lax.all_gather(own_hidden, "kv", axis=1, tiled=True)
    normed_mlp = rms_rows(hidden, mlp_gain)
    squared = jnp.square(jax.nn.relu(jnp.dot(normed_mlp, w_up, preferred_element_type=jnp.float32)))
    squared = squared.astype(jnp.bfloat16)
    partial_mlp = jnp.dot(squared, w_down, preferred_element_type=jnp.float32)
    mlp_part = lax.psum_scatter(partial_mlp, "kv", scatter_dimension=1, tiled=True)
    layer_out = (own_hidden.astype(jnp.float32) + mlp_part).astype(jnp.bfloat16)
    return (layer_out, state_next, value_tail, maps_tail)


def solution(mesh):
    in_specs = (
        P(("dp", "tp"), "kv"),
        P(),
        P(None, "kv"),
        P(None, "kv"),
        P(None, "kv"),
        P(),
        P(None, "kv"),
        P(None, "kv"),
        P(("dp", "tp"), None, "kv"),
        P(("dp", "tp"), None, "kv"),
        P("kv"),
        P("kv"),
        P("kv"),
        P("kv"),
        P(("dp", "tp"), "kv", None, None),
        P("kv", None),
        P(),
        P(None, "kv"),
        P("kv", None),
    )
    out_specs = (
        P(("dp", "tp"), "kv"),
        P(("dp", "tp"), "kv", None, None),
        P(("dp", "tp"), None, "kv"),
        P(("dp", "tp"), None, "kv"),
    )
    peers = mesh.shape["kv"]

    def device_part(*args):
        if kernels_fit(peers, args[0], args[14], args[4], args[17]):
            return local_kernels(peers, *args)
        return local(*args)

    return jax.shard_map(
        device_part, mesh=mesh, in_specs=in_specs, out_specs=out_specs, check_vma=False
    )
```

time: 39.9 us -> 37.1 us (0.930)
  Pallas kernels: 38.5 us -> 36.3 us
  local copies, waits for them, and re-layouts: 0.61 us -> 0 us
    pallas_call x3 -> x2, Pallas kernels: 38.5 us -> 36.3 us  [the longest x1 31.4 us: decode(): pl.pallas_call(functools.partial(decode_kernel, peers), out_shape=(pltpu....]
    unnamed x1 -> x0, local copies, waits for them, and re-layouts: 0.61 us -> none
where the time goes in v2:
time: 37.1 us; the launch traced here: 36.9 us
  Pallas kernels  36.3 us (98%)
  between operations  0.65 us (2%)
    pallas_call x1, Pallas kernels, decode(): pl.pallas_call(functools.partial(decode_kernel, peers), out_shape=(pltpu....  31.4 us
    pallas_call x1, Pallas kernels, flush(): pl.pallas_call(flush_kernel, out_shape=(pltpu.HBM(layer.shape, bf16), plt...  4.94 us

profile of v2, /device:TPU:0, one launch (start us, length us, event | category | flops | bytes accessed | tf_op | source)
XLA Modules:
  0.0 36.9 jit_solution(8291174271111540036)
XLA Ops:
  0.6 31.4 %decode.1 = (bf16[24,512]{1,0:T(8,128)(2,1)S(1)}, bf16[24,1024]{1,0:T(8,128)(2,1)S(1)}, bf16[24,4096]{1,0:T(8,128)(2,1)S(1)}, bf16[3,24,1024]{2,1,0:T(8,128)(2,1...) custom-call(bf16[24,512]{1,0:T(8,128)(2,1)} %tokens_in.1, f32[1,2048]{1,0:T(1,128)} %bitcast.14, ...), custom_call_target="tpu_custom_call" | custom-call | tf_op jit(solution)/shard_map/decode/pallas_call | solution.py:497
  32.0 4.9 %flush.1 = (bf16[24,512]{1,0:T(8,128)(2,1)}, f32[24,16,64,128]{3,2,1,0:T(8,128)}, bf16[3,24,1024]{2,1,0:T(8,128)(2,1)}, bf16[3,24,4096]{2,1,0:T(8,128)(2,1)}) custom-call(bf16[24,512]{1,0:T(8,128)(2,1)S(1)} %get-tuple-element.14.layer, bf16[24,1024]{1,0:T(8,128)(2,1)S(1)} %get-tuple-element.15.value_new, bf16[24,4096]{1,0:T(8,128)(2,1)S(1)} %get-tuple-element.16.maps_new, ...), custom_call_target="tpu_custom_call" | custom-call | tf_op jit(solution)/shard_map/flush/pallas_call | solution.py:588

commit v3 on v2

--- a/solution.py
+++ b/solution.py
@@ -12,6 +12,7 @@
 MESH = pl.DeviceIdType.MESH
 FUSED_LIMIT = 49 * 1024 * 1024
 WINDOW = 9
+SIDES = 2
 
 
 NORM_EPS = 1e-05
@@ -28,18 +29,20 @@
     return other
 
 
-def greet(peers, me):
-    for d in range(1, peers):
-        pl.semaphore_signal(
-            pltpu.get_barrier_semaphore(),
-            inc=1,
-            device_id={"kv": partner(me, d)},
-            device_id_type=MESH,
-        )
+def greet(peers, me, side):
+    for d in range(peers):
+        for t in range(SIDES):
+            if d > 0 or t > 0:
+                pl.semaphore_signal(
+                    pltpu.get_barrier_semaphore(),
+                    inc=1,
+                    device_id={"kv": partner(me, d), "tp": lax.rem(side + t, SIDES)},
+                    device_id_type=MESH,
+                )
 
 
 def all_here(peers):
-    pl.semaphore_wait(pltpu.get_barrier_semaphore(), peers - 1)
+    pl.semaphore_wait(pltpu.get_barrier_semaphore(), SIDES * peers - 1)
 
 
 def far_first(peers):
@@ -52,7 +55,7 @@
         dst_ref=dst,
         send_sem=send_sem,
         recv_sem=recv_sem,
-        device_id={"kv": target},
+        device_id=target,
         device_id_type=MESH,
     )
 
@@ -112,6 +115,13 @@
     conv_value,
     conv_maps,
     slots,
+    twin,
+    give_gate,
+    give_value,
+    give_maps,
+    land_gate,
+    land_value,
+    land_maps,
     weights,
     acc,
     gate,
@@ -119,10 +129,13 @@
     maps_act,
     decay_rows,
     step_cols,
+    skip_cols,
     spread,
     pick,
     readers,
+    direct,
     read,
+    heads_out,
     out_w,
     up_w,
     down_w,
@@ -147,6 +160,10 @@
     recv_h,
     send_b,
     recv_b,
+    send_f,
+    recv_f,
+    send_x,
+    recv_x,
 ):
     me = lax.axis_index("kv")
     rows, part = tokens.shape
@@ -157,7 +174,8 @@
     wide = 4 * STATE
     taps = past_value.shape[0]
     pairs = heads // 2
-    greet(peers, me)
+    side = lax.axis_index("tp")
+    greet(peers, me, side)
 
     def place(d):
         return pl.multiple_of(partner(me, d) * part, part)
@@ -182,21 +200,25 @@
         )
     ]
 
+    half = inner // 2
+    half_at = pl.ds(pl.multiple_of(side * half, half), half)
+
+    def maps_at(t, c):
+        return pl.ds(pl.multiple_of(t * 2 * width + (c - 1) * width, width), width)
+
     def weight_copies(d, c):
         if c == 0:
             return [
                 pltpu.make_async_copy(
-                    ref.at[pl.ds(place(d), part), :],
-                    weights.at[d, 0, :, pl.ds(k * inner, inner)],
+                    ref.at[pl.ds(place(d), part), half_at],
+                    weights.at[d, 0, :, pl.ds(k * half, half)],
                     w_sem.at[d, 0],
                 )
                 for k, ref in enumerate((w_gate, w_value))
             ]
         return [
             pltpu.make_async_copy(
-                w_maps.at[pl.ds(place(d), part), pl.ds((c - 1) * width, width)],
-                weights.at[d, c],
-                w_sem.at[d, c],
+                w_maps.at[pl.ds(place(d), part), maps_at(side, c)], weights.at[d, c], w_sem.at[d, c]
             )
         ]
 
@@ -235,16 +257,19 @@
     all_here(peers)
     pending = []
 
-    def send(src, dst, send_sem, recv_sem, d):
-        cp = push(src, dst, send_sem.at[d], recv_sem.at[d], partner(me, d))
+    def send(src, dst, send_sem, recv_sem, d, t):
+        cp = push(src, dst, send_sem, recv_sem, {"kv": partner(me, d), "tp": t})
         cp.start()
-        pending.append(cp)
-
-    def arrived(src, dst, send_sem, recv_sem, d):
-        push(src, dst, send_sem.at[d], recv_sem.at[d], me).wait_recv()
+        return cp
+
+    def arrived(dst, recv_sem):
+        push(dst, dst, recv_sem, recv_sem, {"kv": me, "tp": side}).wait_recv()
 
     for d in far_first(peers):
-        send(tokens, slots.at[d], send_t, recv_t, d)
+        pending.append(send(tokens, slots.at[d], send_t.at[d], recv_t.at[d], d, side))
+
+    facing = lax.rem(side + 1, SIDES)
+    pending.append(send(tokens, twin.at[0], send_f.at[0], recv_f.at[0], 0, facing))
     for cp in small[3:]:
         cp.start()
     load(WINDOW - chunks)
@@ -256,146 +281,160 @@
     def by_head(table, h):
         return jnp.where(lane < HEAD_DIM, table[:, h : h + 1], table[:, h + 1 : h + 2])
 
-    squares = jnp.zeros((rows, 1), jnp.float32)
-    step_pre = jnp.zeros((2 * rows, w_step.shape[0]), jnp.float32)
+    both = SIDES * rows
+    squares = jnp.zeros((both, 1), jnp.float32)
+    step_pre = jnp.zeros((2 * both, w_step.shape[0]), jnp.float32)
     for d in range(peers):
         if d == 0:
-            raw = tokens[...]
+            ahead = [1] if peers > 1 else []
         else:
-            arrived(tokens, slots.at[d], send_t, recv_t, d)
-            raw = slots[d]
-        x = raw.astype(jnp.float32)
+            ahead = [d + 1] if d + 1 < peers else []
+        arrived(twin.at[d], recv_f.at[d])
+        raw = [tokens[...] if d == 0 else slots[d], twin[d]]
+        x = jnp.concatenate([half_rows.astype(jnp.float32) for half_rows in raw], axis=0)
         squares = squares + jnp.sum(x * x, axis=1, keepdims=True)
         scaled = jnp.concatenate(split(x * gain[:, pl.ds(place(d), part)]), axis=0)
         scaled = scaled.astype(jnp.bfloat16)
         step_pre = step_pre + lax.dot_general(
             scaled, w_step[:, pl.ds(place(d), part)], NT, preferred_element_type=jnp.float32
         )
+        for e in ahead:
+            arrived(slots.at[e], recv_t.at[e])
+            pending.append(send(slots.at[e], twin.at[e], send_f.at[e], recv_f.at[e], 0, facing))
         last = d == peers - 1
         if last:
             inv = lax.rsqrt(squares / (peers * part) + NORM_EPS)
-            step_pre = (step_pre[:rows] + step_pre[rows:]) * inv
-            own = step_pre[:, :heads]
-            for j in range(1, peers):
-                own = jnp.where(me == j, step_pre[:, j * heads : (j + 1) * heads], own)
-            own = own + bias[...]
-            step = jnp.maximum(own, 0.0) + jnp.log1p(jnp.exp(-jnp.abs(own)))
-            decay = jnp.exp(-step * jnp.exp(decay_log[...]))
-            for h in range(heads):
-                decay_rows[h] = jnp.broadcast_to(decay[:, h : h + 1], (rows, STATE))
-            for h in range(0, heads, 2):
-                step_cols[:, h * HEAD_DIM : (h + 2) * HEAD_DIM] = by_head(step, h)
-
         for c in range(chunks):
             pltpu.make_async_copy(
                 w_maps.at[pl.ds(0, part), pl.ds(0, width)], weights.at[d, c], w_sem.at[d, c]
             ).wait()
             load(1)
             out = jnp.dot(scaled, weights[d, c], preferred_element_type=jnp.float32)
-            out = out[:rows] + out[rows:]
+            out = out[:both] + out[both:]
             total = out if d == 0 else acc[c] + out
             if not last:
                 acc[c] = total
                 continue
             total = total * inv
-
-            def conv(new, past, at, cols, table):
-                summed = new.astype(jnp.float32) * table[taps : taps + 1, at : at + cols]
-                for k in range(taps):
-                    row = past[k, :, at : at + cols].astype(jnp.float32)
-                    summed = summed + row * table[k : k + 1, at : at + cols]
-                return silu(summed)
-
             if c == 0:
-                gate[...] = silu(total[:, :inner])
-                new = total[:, inner:].astype(jnp.bfloat16)
-                value_new[...] = new
-                value_act[...] = conv(new, past_value, 0, inner, conv_value)
+                gate[:, half_at] = total[:rows, :half]
+                value_new[:, half_at] = total[:rows, half:].astype(jnp.bfloat16)
+                give_gate[...] = total[rows:, :half]
+                give_value[...] = total[rows:, half:].astype(jnp.bfloat16)
+                pending.append(send(give_gate, land_gate, send_x.at[c], recv_x.at[c], 0, facing))
+                pending.append(
+                    send(
+                        give_value, land_value, send_x.at[chunks], recv_x.at[chunks], 0, facing
+                    )
+                )
             else:
-                at = (c - 1) * width
-                new = total.astype(jnp.bfloat16)
-                maps_new[:, at : at + width] = new
-                act = conv(new, past_maps, at, width, conv_maps)
-                maps_act[:, at : at + width] = act.astype(jnp.bfloat16)
+                maps_new[:, maps_at(side, c)] = total[:rows].astype(jnp.bfloat16)
+                give_maps[c] = total[rows:].astype(jnp.bfloat16)
+                pending.append(
+                    send(give_maps.at[c], land_maps.at[c], send_x.at[c], recv_x.at[c], 0, facing)
+                )
+
+    step_pre = (step_pre[:rows] + step_pre[both : both + rows]) * inv[:rows]
+    own = step_pre[:, :heads]
+    for j in range(1, peers):
+        own = jnp.where(me == j, step_pre[:, j * heads : (j + 1) * heads], own)
+    own = own + bias[...]
+    step = jnp.maximum(own, 0.0) + jnp.log1p(jnp.exp(-jnp.abs(own)))
+    decay = jnp.exp(-step * jnp.exp(decay_log[...]))
+    for h in range(heads):
+        decay_rows[h] = jnp.broadcast_to(decay[:, h : h + 1], (rows, STATE))
+    for h in range(0, heads, 2):
+        step_cols[:, h * HEAD_DIM : (h + 2) * HEAD_DIM] = by_head(step, h)
+
+    for h in range(0, heads, 2):
+        skip_cols[:, h * HEAD_DIM : (h + 2) * HEAD_DIM] = by_head(skip, h)
+
+    def conv(fresh, past, cols, table):
+        summed = fresh[:, cols].astype(jnp.float32) * table[taps : taps + 1, cols]
+        for k in range(taps):
+            old = past[k, :, cols].astype(jnp.float32)
+            summed = summed + old * table[k : k + 1, cols]
+        return silu(summed)
 
     row = lax.broadcasted_iota(jnp.int32, (2 * rows, STATE), 0)
     column = lax.broadcasted_iota(jnp.int32, (2 * rows, STATE), 1)
     seq = jnp.where(row >= rows, row - rows, row)
     owner = jnp.where((row >= rows) == (column >= HEAD_DIM), seq, -1)
     read[...] = jnp.zeros_like(read)
-
-    for i in range(pairs):
-        at = i * wide
-        readers[i] = jnp.concatenate(
-            [
-                maps_act[:, at + STATE : at + 2 * STATE].astype(jnp.float32),
-                maps_act[:, at + 3 * STATE : at + wide].astype(jnp.float32),
-            ],
-            axis=0,
-        ).astype(jnp.bfloat16)
+    early = lax.rem(seq, 4) < 2
+    first = lane < HEAD_DIM
+
+    def ready(t):
+        cols = pl.ds(pl.multiple_of(t * half, half), half)
+        gate[:, cols] = silu(gate[:, cols])
+        value_act[:, cols] = conv(value_new, past_value, cols, conv_value)
+        for c in range(1, chunks):
+            cols = maps_at(t, c)
+            maps_act[:, cols] = conv(maps_new, past_maps, cols, conv_maps).astype(jnp.bfloat16)
+        for k in range(pairs // 2):
+            i = t * (pairs // 2) + k
+            maps = maps_act[:, pl.ds(pl.multiple_of(i * wide, wide), wide)].astype(jnp.float32)
+            outof = [maps[:, m * STATE : (m + 1) * STATE] for m in range(4)]
+            stacked = jnp.concatenate([outof[1], outof[3]], axis=0)
+            readers[i] = jnp.concatenate(
+                [jnp.where(early, stacked, 0.0), jnp.where(early, 0.0, stacked)], axis=1
+            ).astype(jnp.bfloat16)
+            at = pl.ds(pl.multiple_of(i * pair, pair), pair)
+            act = value_act[:, at]
+            dots = [jnp.sum(outof[m] * outof[m + 1], axis=1, keepdims=True) for m in (0, 2)]
+            dots = jnp.where(first, dots[0], dots[1])
+            direct[:, at] = dots * (act * step_cols[:, at]) + skip_cols[:, at] * act
 
     def read_pair(i, r):
+        strips = []
+        for k in range(2):
+            for hh in range(2):
+                h = 2 * i + hh
+                strips.append(
+                    jnp.concatenate(
+                        [state[r * block + k, h], state[r * block + k + 2, h]], axis=1
+                    ).astype(jnp.bfloat16)
+                )
+        found = lax.dot_general(
+            readers[i], jnp.concatenate(strips, axis=0), NT, preferred_element_type=jnp.float32
+        )
         total = read[i]
-        for k0 in range(0, block, 2):
-            tiles = []
-            for k in range(k0, k0 + 2):
-                for hh in range(2):
-                    tiles.append(state[r * block + k, 2 * i + hh].astype(jnp.bfloat16))
-            found = lax.dot_general(
-                readers[i], jnp.concatenate(tiles, axis=0), NT, preferred_element_type=jnp.float32
-            )
-            for k in range(2):
-                total = total + jnp.where(
-                    owner == r * block + k0 + k, found[:, k * pair : (k + 1) * pair], 0.0
-                )
+        for k in range(2):
+            hit = (owner == r * block + k) | (owner == r * block + k + 2)
+            total = total + jnp.where(hit, found[:, k * pair : (k + 1) * pair], 0.0)
         read[i] = total
 
+    ready(side)
     for r in range(blocks):
         state_copy(r).wait()
         load(1)
-        for i in range(pairs):
-            read_pair(i, r)
+        for k in range(pairs // 2):
+            read_pair(side * (pairs // 2) + k, r)
     load(len(bulk))
-
-    heads_out = []
-    first = lane < HEAD_DIM
+    facing_half = pl.ds(pl.multiple_of(facing * half, half), half)
+    arrived(land_gate, recv_x.at[0])
+    gate[:, facing_half] = land_gate[...]
+    arrived(land_value, recv_x.at[chunks])
+    value_new[:, facing_half] = land_value[...]
+    for c in range(1, chunks):
+        arrived(land_maps.at[c], recv_x.at[c])
+        maps_new[:, maps_at(facing, c)] = land_maps[c]
+    ready(facing)
+    for r in range(blocks):
+        for k in range(pairs // 2):
+            read_pair(facing * (pairs // 2) + k, r)
+
     for i in range(pairs):
         at = slice(i * pair, (i + 1) * pair)
-        act = value_act[:, at]
-        scaled = act * step_cols[:, at]
-        inner_dots = []
-        for hh in range(2):
-            m = i * wide + 2 * hh * STATE
-            into = maps_act[:, m : m + STATE].astype(jnp.float32)
-            outof = maps_act[:, m + STATE : m + 2 * STATE].astype(jnp.float32)
-            inner_dots.append(jnp.sum(into * outof, axis=1, keepdims=True))
         h = 2 * i
         decayed = jnp.where(first, decay_rows[h], decay_rows[h + 1])
         found = read[i]
-        read_out = decayed * (found[:rows] + found[rows:])
-        read_out = read_out + jnp.where(first, inner_dots[0], inner_dots[1]) * scaled
-        gated = (read_out + by_head(skip, h) * act) * gate[:, at]
+        gated = (decayed * (found[:rows] + found[rows:]) + direct[:, at]) * gate[:, at]
         square = gated * gated
         low = jnp.sum(jnp.where(first, square, 0.0), axis=1, keepdims=True)
         top = jnp.sum(jnp.where(first, 0.0, square), axis=1, keepdims=True)
         norm = lax.rsqrt(jnp.where(first, low, top) / HEAD_DIM + NORM_EPS)
-        heads_out.append((gated * norm * head_gain[:, at]).astype(jnp.bfloat16))
-    heads_out = jnp.concatenate(heads_out, axis=1)
-
-    def scatter(left, waits, weight, sums, land, send_sem, recv_sem, between):
-        for d in order:
-            waits[d].wait()
-            piece = jnp.dot(left, weight[d], preferred_element_type=jnp.float32)
-            if d == 0:
-                total = piece
-            else:
-                sums[d] = piece.astype(jnp.bfloat16)
-                send(sums.at[d], land.at[d], send_sem, recv_sem, d)
-        between()
-        for d in range(1, peers):
-            arrived(sums.at[d], land.at[d], send_sem, recv_sem, d)
-            total = total + land[d].astype(jnp.float32)
-        return total
+        heads_out[:, at] = (gated * norm * head_gain[:, at]).astype(jnp.bfloat16)
 
     def prepare():
         spot = lax.broadcasted_iota(jnp.int32, (16, STATE), 1)
@@ -439,43 +478,98 @@
                     )
         return carry
 
-    def first_half():
+    def out_piece(d):
+        outs[d].wait()
+        return jnp.dot(heads_out[...], out_w[d], preferred_element_type=jnp.float32)
+
+    def give_sums(t, targets):
+        sent = []
+        for d in targets:
+            sums_a[d] = out_piece(d).astype(jnp.bfloat16)
+            sent.append(
+                send(sums_a.at[d], land_a.at[t, d], send_a.at[d], recv_a.at[t, d], d, 1)
+            )
+        return sent
+
+    @pl.when(side == 0)
+    def _():
+        sent = give_sums(0, order)
+        prepare()
+        lax.fori_loop(0, pairs, update, 0)
+        arrived(own_hidden.at[0], recv_h.at[0])
+        total = own_hidden[0].astype(jnp.float32)
+        for d in range(peers):
+            arrived(land_b.at[d], recv_b.at[d])
+            total = total + land_b[d].astype(jnp.float32)
+        layer_out[...] = total.astype(jnp.bfloat16)
+        for cp in sent:
+            cp.wait_send()
+
+    @pl.when(side == 1)
+    def _():
+        sent = give_sums(1, far_first(peers))
+        mine = tokens[...].astype(jnp.float32) + out_piece(0)
         for cp in ups:
             cp.start(priority=1)
         prepare()
         lax.fori_loop(0, pairs // 2, update, 0)
-
-    total = scatter(heads_out, outs, out_w, sums_a, land_a, send_a, recv_a, first_half)
-    mine = (tokens[...].astype(jnp.float32) + total).astype(jnp.bfloat16)
-    own_hidden[...] = mine
-    for d in far_first(peers):
-        send(own_hidden, hidden.at[d], send_h, recv_h, d)
-    for d in order:
-        downs[d].start(priority=1)
-    lax.fori_loop(pairs // 2, pairs, update, 0)
-
-    squares = jnp.zeros((rows, 1), jnp.float32)
-    for d in range(peers):
-        if d == 0:
-            raw = mine
-        else:
-            arrived(own_hidden, hidden.at[d], send_h, recv_h, d)
-            raw = hidden[d]
-        x = raw.astype(jnp.float32)
-        squares = squares + jnp.sum(x * x, axis=1, keepdims=True)
-        scaled = jnp.concatenate(split(x * mlp_gain[:, pl.ds(place(d), part)]), axis=0)
-        ups[d].wait()
-        out = jnp.dot(scaled.astype(jnp.bfloat16), up_w[d], preferred_element_type=jnp.float32)
-        out = out[:rows] + out[rows:]
-        up = out if d == 0 else up + out
-
-    inv = lax.rsqrt(squares / (peers * part) + NORM_EPS)
-    up = jnp.maximum(up * inv, 0.0)
-    squared[...] = (up * up).astype(jnp.bfloat16)
-    total = scatter(
-        squared[...], downs, down_w, sums_b, land_b, send_b, recv_b, lambda: None
-    )
-    layer_out[...] = (mine.astype(jnp.float32) + total).astype(jnp.bfloat16)
+        other = twin[0].astype(jnp.float32)
+        for d in range(peers):
+            if d > 0:
+                arrived(land_a.at[1, d], recv_a.at[1, d])
+                mine = mine + land_a[1, d].astype(jnp.float32)
+            arrived(land_a.at[0, d], recv_a.at[0, d])
+            other = other + land_a[0, d].astype(jnp.float32)
+        own_hidden[0] = other.astype(jnp.bfloat16)
+        own_hidden[1] = mine.astype(jnp.bfloat16)
+        for d in far_first(peers):
+            sent.append(send(own_hidden, hidden.at[d], send_h.at[d], recv_h.at[d], d, 1))
+        sent.append(
+            send(own_hidden.at[0], own_hidden.at[0], send_h.at[0], recv_h.at[0], 0, 0)
+        )
+        for d in order:
+            downs[d].start(priority=1)
+        lax.fori_loop(pairs // 2, pairs, update, 0)
+
+        squares = jnp.zeros((both, 1), jnp.float32)
+        for d in range(peers):
+            if d == 0:
+                raw = [own_hidden[t] for t in range(SIDES)]
+            else:
+                arrived(hidden.at[d], recv_h.at[d])
+                raw = [hidden[d, t] for t in range(SIDES)]
+            x = jnp.concatenate([part_t.astype(jnp.float32) for part_t in raw], axis=0)
+            squares = squares + jnp.sum(x * x, axis=1, keepdims=True)
+            scaled = jnp.concatenate(split(x * mlp_gain[:, pl.ds(place(d), part)]), axis=0)
+            ups[d].wait()
+            out = jnp.dot(scaled.astype(jnp.bfloat16), up_w[d], preferred_element_type=jnp.float32)
+            out = out[:both] + out[both:]
+            up = out if d == 0 else up + out
+
+        inv = lax.rsqrt(squares / (peers * part) + NORM_EPS)
+        up = jnp.maximum(up * inv, 0.0)
+        squared[...] = (up * up).astype(jnp.bfloat16)
+        for d in order:
+            downs[d].wait()
+            piece = jnp.dot(squared[...], down_w[d], preferred_element_type=jnp.float32)
+            sums_b[0, d] = piece[:rows].astype(jnp.bfloat16)
+            sent.append(
+                send(sums_b.at[0, d], land_b.at[d], send_b.at[0, d], recv_b.at[d], d, 0)
+            )
+            if d > 0:
+                sums_b[1, d] = piece[rows:].astype(jnp.bfloat16)
+                sent.append(
+                    send(sums_b.at[1, d], land_b.at[d], send_b.at[1, d], recv_b.at[d], d, 1)
+                )
+            else:
+                total = own_hidden[1].astype(jnp.float32) + piece[rows:]
+        for d in range(1, peers):
+            arrived(land_b.at[d], recv_b.at[d])
+            total = total + land_b[d].astype(jnp.float32)
+        layer_out[...] = total.astype(jnp.bfloat16)
+        for cp in sent:
+            cp.wait_send()
+
     for cp in pending:
         cp.wait_send()
 
@@ -485,14 +579,16 @@
     heads = state.shape[1]
     inner, maps = heads * HEAD_DIM, 2 * heads * STATE
     hid = later[1].shape[1]
-    width = 2 * inner
-    chunks = 1 + maps // width
+    width = inner
+    chunks = 1 + maps // (2 * width)
     f32, bf16 = jnp.float32, jnp.bfloat16
-    block = 4 if rows % 4 == 0 else 2
+    block = 4
     vmem = pl.BlockSpec(memory_space=pltpu.VMEM)
     hbm = pl.BlockSpec(memory_space=pl.ANY)
     sems = pltpu.SemaphoreType.DMA((peers,))
     slots = pltpu.VMEM((peers, rows, part), bf16)
+    both_slots = pltpu.VMEM((SIDES, peers, rows, part), bf16)
+    both_sems = pltpu.SemaphoreType.DMA((SIDES, peers))
     operands = (tokens, *small, past_value, past_maps, *weights, state, *later)
     return pl.pallas_call(
         functools.partial(decode_kernel, peers),
@@ -510,31 +606,55 @@
             pltpu.VMEM((rows, part), bf16),
             *[pltpu.VMEM(x.shape, x.dtype) for x in small],
             slots,
+            slots,
+            pltpu.VMEM((rows, inner // 2), f32),
+            pltpu.VMEM((rows, inner // 2), bf16),
+            pltpu.VMEM((chunks, rows, width), bf16),
+            pltpu.VMEM((rows, inner // 2), f32),
+            pltpu.VMEM((rows, inner // 2), bf16),
+            pltpu.VMEM((chunks, rows, width), bf16),
             pltpu.VMEM((peers, chunks, part, width), bf16),
-            pltpu.VMEM((chunks, rows, width), f32),
+            pltpu.VMEM((chunks, SIDES * rows, width), f32),
             pltpu.VMEM((rows, inner), f32),
             pltpu.VMEM((rows, inner), f32),
             pltpu.VMEM((rows, maps), bf16),
             pltpu.VMEM((heads, rows, STATE), f32),
             pltpu.VMEM((rows, inner), f32),
+            pltpu.VMEM((rows, inner), f32),
             pltpu.VMEM((heads // 2, HEAD_DIM, STATE), bf16),
             pltpu.VMEM((rows, 16, STATE), bf16),
-            pltpu.VMEM((heads // 2, 2 * rows, STATE), bf16),
+            pltpu.VMEM((heads // 2, 2 * rows, 2 * STATE), bf16),
+            pltpu.VMEM((rows, inner), f32),
             pltpu.VMEM((heads // 2, 2 * rows, STATE), f32),
+            pltpu.VMEM((rows, inner), bf16),
             pltpu.VMEM((peers, inner, part), bf16),
             pltpu.VMEM((peers, part, hid), bf16),
             pltpu.VMEM((peers, hid, part), bf16),
             slots,
-            slots,
-            pltpu.VMEM((rows, part), bf16),
-            slots,
-            pltpu.VMEM((rows, hid), bf16),
-            slots,
+            both_slots,
+            pltpu.VMEM((SIDES, rows, part), bf16),
+            pltpu.VMEM((peers, SIDES, rows, part), bf16),
+            pltpu.VMEM((SIDES * rows, hid), bf16),
+            both_slots,
             slots,
             pltpu.SemaphoreType.DMA((12,)),
             pltpu.SemaphoreType.DMA((peers, chunks)),
             pltpu.SemaphoreType.DMA((rows // block,)),
-            *[sems] * 11,
+            sems,
+            sems,
+            sems,
+            sems,
+            sems,
+            sems,
+            both_sems,
+            sems,
+            sems,
+            both_sems,
+            sems,
+            sems,
+            sems,
+            pltpu.SemaphoreType.DMA((chunks + 1,)),
+            pltpu.SemaphoreType.DMA((chunks + 1,)),
         ],
         compiler_params=pltpu.CompilerParams(
             collective_id=0, has_side_effects=True, vmem_limit_bytes=FUSED_LIMIT
@@ -651,7 +771,7 @@
     return layer_out, state_next, jnp.swapaxes(tail_v, 0, 1), jnp.swapaxes(tail_m, 0, 1)
 
 
-def kernels_fit(peers, tokens, state, w_maps, w_up):
+def kernels_fit(peers, sides, tokens, state, w_maps, w_up):
     rows, part = tokens.shape
     heads = state.shape[1]
     inner = heads * HEAD_DIM
@@ -660,6 +780,7 @@
     held = 4 * rows * heads * HEAD_DIM * STATE
     return (
         peers > 1
+        and sides == SIDES
         and peers & (peers - 1) == 0
         and rows % 8 == 0
         and 4 * rows <= STATE
@@ -781,7 +902,7 @@
     peers = mesh.shape["kv"]
 
     def device_part(*args):
-        if kernels_fit(peers, args[0], args[14], args[4], args[17]):
+        if kernels_fit(peers, mesh.shape["tp"], args[0], args[14], args[4], args[17]):
             return local_kernels(peers, *args)
         return local(*args)
 

time: 37.1 us -> 35.8 us (0.965)
  Pallas kernels: 36.3 us -> 35 us
    pallas_call x1, Pallas kernels: 31.4 us -> 30 us  [decode(): pl.pallas_call(functools.partial(decode_kernel, peers), out_shape=(pltpu....]
where the time goes in v3:
time: 35.8 us; the launch traced here: 35.6 us
  Pallas kernels  35 us (98%)
  between operations  0.65 us (2%)
    pallas_call x1, Pallas kernels, decode(): pl.pallas_call(functools.partial(decode_kernel, peers), out_shape=(pltpu....  30 us
    pallas_call x1, Pallas kernels, flush(): pl.pallas_call(flush_kernel, out_shape=(pltpu.HBM(layer.shape, bf16), plt...  4.94 us

profile of v3, /device:TPU:0, one launch (start us, length us, event | category | flops | bytes accessed | tf_op | source)
XLA Modules:
  0.0 35.6 jit_solution(4349623106589961583)
XLA Ops:
  0.6 30.0 %decode.1 = (bf16[24,512]{1,0:T(8,128)(2,1)S(1)}, bf16[24,1024]{1,0:T(8,128)(2,1)S(1)}, bf16[24,4096]{1,0:T(8,128)(2,1)S(1)}, bf16[3,24,1024]{2,1,0:T(8,128)(2,1...) custom-call(bf16[24,512]{1,0:T(8,128)(2,1)} %tokens_in.1, f32[1,2048]{1,0:T(1,128)} %bitcast.14, ...), custom_call_target="tpu_custom_call" | custom-call | tf_op jit(solution)/shard_map/decode/pallas_call | solution.py:593
  30.7 4.9 %flush.1 = (bf16[24,512]{1,0:T(8,128)(2,1)}, f32[24,16,64,128]{3,2,1,0:T(8,128)}, bf16[3,24,1024]{2,1,0:T(8,128)(2,1)}, bf16[3,24,4096]{2,1,0:T(8,128)(2,1)}) custom-call(bf16[24,512]{1,0:T(8,128)(2,1)S(1)} %get-tuple-element.14.layer, bf16[24,1024]{1,0:T(8,128)(2,1)S(1)} %get-tuple-element.15.value_new, bf16[24,4096]{1,0:T(8,128)(2,1)S(1)} %get-tuple-element.16.maps_new, ...), custom_call_target="tpu_custom_call" | custom-call | tf_op jit(solution)/shard_map/flush/pallas_call | solution.py:708
